TPU v7x, 128 devices: a whole 4x4x4 slice. The times are simulated.
128 devices in a mesh: ep: 128 (over z, y, x, core).
Axes of the slice: x: 4, y: 4, z: 4, core: 2. Of those that a mesh axis runs over, the one named last changes fastest.
Arguments:
- tokens: bfloat16 [2048, 1024], P('ep'), may hold values from -6 to 6
- lengths: int32 [2048], P('ep'), may hold values from 1 to 8191
- cache_keys: bfloat16 [2048, 128, 512], P('ep'), may hold values from -6 to 6
- cache_values: bfloat16 [2048, 128, 1024], P('ep'), may hold values from -6 to 6
- retention_state: float32 [2048, 4, 128, 256], P('ep'), may hold values from -24 to 24
- mix_gain: float32 [1024], replicated, may hold values from 0.1 to 1.9
- query_weight: bfloat16 [1024, 512], replicated, may hold values from -0.1875 to 0.1875
- key_weight: bfloat16 [1024, 512], replicated, may hold values from -0.1875 to 0.1875
- value_weight: bfloat16 [1024, 1024], replicated, may hold values from -0.1875 to 0.1875
- out_weight: bfloat16 [1024, 1024], replicated, may hold values from -0.1875 to 0.1875
- ffn_gain: float32 [1024], replicated, may hold values from 0.1 to 1.9
- routes: int32 [2048, 6], P('ep'), may hold values from 0 to 127, all different within a row; in each aligned block of 16 rows (0 to 15, 16 to 31, ...) at most 2 rows name the same one
- route_scores: float32 [2048, 6], P('ep'), may hold values from 0.05 to 1
- expert_gate: bfloat16 [128, 1024, 256], P('ep'), may hold values from -0.1875 to 0.1875
- expert_up: bfloat16 [128, 1024, 256], P('ep'), may hold values from -0.1875 to 0.1875
- expert_down: bfloat16 [128, 256, 1024], P('ep'), may hold values from -0.375 to 0.375
- shared_gate: bfloat16 [1024, 256], replicated, may hold values from -0.1875 to 0.1875
- shared_up: bfloat16 [1024, 256], replicated, may hold values from -0.1875 to 0.1875
- shared_down: bfloat16 [256, 1024], replicated, may hold values from -0.375 to 0.375
- dense_gate: bfloat16 [4096, 1024], P('ep'), may hold values from -0.1875 to 0.1875
- dense_up: bfloat16 [4096, 1024], P('ep'), may hold values from -0.1875 to 0.1875
- dense_down: bfloat16 [4096, 1024], P('ep'), may hold values from -0.09375 to 0.09375
- dense_mix: float32 [1024], replicated, may hold values from -3 to 3
Outputs:
- layer_out: bfloat16 [2048, 1024], P('ep')
- new_keys: bfloat16 [2048, 512], P('ep')
- new_values: bfloat16 [2048, 1024], P('ep')
Inputs may be any that keep to these rules, and one draw needn't show every extreme that they name: `routes`: each row names 6 different experts; among the rows of one device no expert is named more than 2 times.
All inputs are finite; a program needn't handle non-finite values.
Results may differ from a plain program's by a relative error of at most 0.012.
Values may be sent and summed in bfloat16 or wider, within the bound.
No kernel may reach another device: no remote copies, remote signals or barrier semaphores. Data moves between devices by JAX's collectives and lax.ppermute only.
A program may use at most 128 MiB of HBM per device.

v0:
```python
import math

import jax
import jax.numpy as jnp
from jax import lax
from jax.experimental import pallas as pl
from jax.experimental.pallas import tpu as pltpu
from jax.sharding import PartitionSpec as P


eps = 1e-06
route_scale = 2.5
rope_base = 10000.0

SEQ = 16
WIDTH = 1024
HEADS = 4
KEY = 128
VALUE = 256
BLOCK = 128
EXPERTS = 128
SLOTS = 2
NEAR = 8
FAR = 16
HELD = SLOTS * NEAR
ROWS = FAR * HELD
GROUP = 4
MIB = 1024 * 1024

near_masks = (6, 24, 96)
far_masks = (1, 2, 8, 32)

f32 = jnp.float32
bf16 = jnp.bfloat16
vmem = pl.BlockSpec(memory_space=pltpu.VMEM)
hbm = pl.BlockSpec(memory_space=pltpu.HBM)


def flip(values, mask):
    return lax.ppermute(values, "ep", [(i, i ^ mask) for i in range(lax.axis_size("ep"))])


def normed(values):
    return values * lax.rsqrt(jnp.mean(values * values, axis=-1, keepdims=True) + eps)


def dot(a, b):
    return jnp.dot(a, b, preferred_element_type=f32)


def dot_t(a, b):
    return lax.dot_general(a, b, (((1,), (1,)), ((), ())), preferred_element_type=f32)


def dot_0(a, b):
    return lax.dot_general(a, b, (((0,), (0,)), ((), ())), preferred_element_type=f32)


def iota(shape, axis):
    return lax.broadcasted_iota(jnp.int32, shape, axis)


def silu(v):
    return v / (1.0 + jnp.exp(-v))


def head_rates(head_ids):
    return jnp.log1p(-jnp.exp2(-5.0 - head_ids.astype(f32)))


def rotary(length_of):
    shape = (SEQ, KEY)
    row = iota(shape, 0)
    half = KEY // 2
    position = jnp.zeros(shape, f32)
    for s in range(SEQ):
        position = jnp.where(row == s, length_of(s).astype(f32), position)
    lane = iota(shape, 1)
    inverse = jnp.exp((lane % half).astype(f32) * (-math.log(rope_base) / half))
    angles = position * inverse
    sine = jnp.sin(angles)
    return jnp.cos(angles), jnp.where(lane < half, -sine, sine)


def route_weights(routes, scores):
    expert = iota((EXPERTS, SEQ), 0)
    weight = scores / jnp.sum(scores, axis=0, keepdims=True) * route_scale
    weighted = jnp.zeros((EXPERTS, SEQ), f32)
    for k in range(routes.shape[0]):
        weighted = jnp.where(routes[k : k + 1, :] == expert, weight[k : k + 1, :], weighted)
    same = (iota((EXPERTS, EXPERTS), 0) == iota((EXPERTS, EXPERTS), 1)).astype(bf16)
    return dot_0(weighted.astype(bf16), same).astype(bf16)


def mixer_kernel(
    lengths_h,
    routes_h,
    scores_h,
    tokens_h,
    mix_gain_h,
    wq_h,
    wk_h,
    keys_h,
    wv_h,
    ffn_gain_h,
    wo_h,
    values_h,
    state_h,
    gate_h,
    up_h,
    down_h,
    residual_o,
    ffn_o,
    new_keys_o,
    new_values_o,
    outgoing_o,
    shard_o,
    lengths_s,
    routes_s,
    scores_s,
    tokens_s,
    mix_gain,
    wq,
    wk,
    keys,
    wv,
    ffn_gain,
    wo,
    values,
    state,
    weights_s,
    retained_s,
    sems,
    group_sems,
    shard_sems,
):
    sources = (
        lengths_h, routes_h, scores_h, tokens_h, mix_gain_h, wq_h, wk_h, keys_h, wv_h, ffn_gain_h, wo_h
    )
    targets = (
        lengths_s, routes_s, scores_s, tokens_s, mix_gain, wq, wk, keys, wv, ffn_gain, wo
    )
    copies = [
        pltpu.make_async_copy(src, dst, sems.at[i])
        for i, (src, dst) in enumerate(zip(sources, targets))
    ]
    steps = SEQ // GROUP
    group_copies = []
    for g in range(steps):
        part = pl.ds(g * GROUP, GROUP)
        group_copies.append(
            (
                pltpu.make_async_copy(values_h.at[part], values.at[part], group_sems.at[0, g]),
                pltpu.make_async_copy(state_h.at[part], state.at[part], group_sems.at[1, g]),
            )
        )
    for c in copies[:8]:
        c.start()
    for c in group_copies[0]:
        c.start()
    for c in copies[8:10]:
        c.start()
    for pair in group_copies[1:]:
        for c in pair:
            c.start()
    copies[10].start()
    rows = gate_h.shape[0]
    shard_copies = [
        pltpu.make_async_copy(src, shard_o.at[pl.ds(i * rows, rows)], shard_sems.at[i])
        for i, src in enumerate((gate_h, up_h, down_h))
    ]
    for c in shard_copies:
        c.start()
    for c in copies[:3]:
        c.wait()

    def filled_of(s):
        return lax.rem(lengths_s[s], BLOCK)

    route_weight = route_weights(routes_s[...], scores_s[...])

    cosine, sine = rotary(lambda s: lengths_s[s])
    cos = jnp.concatenate([cosine] * HEADS, axis=1)
    sin = jnp.concatenate([sine] * HEADS, axis=1)
    copies[3].wait()
    copies[4].wait()
    widened = tokens_s[...].astype(f32)
    normal_in = (normed(widened) * mix_gain[...]).astype(bf16)

    def rotate(raw):
        swapped = jnp.concatenate(
            [pltpu.roll(raw[:, h * KEY : (h + 1) * KEY], KEY // 2, 1) for h in range(HEADS)],
            axis=1,
        )
        return raw * cos + swapped * sin

    copies[5].wait()
    copies[6].wait()
    queries = (rotate(dot(normal_in, wq[...])) * KEY ** (-0.5)).astype(bf16)
    new_keys = rotate(dot(normal_in, wk[...])).astype(bf16)
    new_keys_o[...] = new_keys
    queries32 = queries.astype(f32)
    product = queries32 * new_keys.astype(f32)

    head_of = iota((8, HEADS * KEY), 0)
    query_block = iota((8, HEADS * KEY), 1) // KEY == head_of
    place = iota((8, BLOCK), 1)
    rate_wide = head_rates(iota((8, BLOCK), 0))
    rate_tall = head_rates(iota((8, 1), 0))
    value_block = iota((8, HEADS * VALUE), 1) // VALUE == iota((8, HEADS * VALUE), 0)

    blocked = []
    copies[7].wait()
    for s in range(SEQ):
        spread_query = jnp.where(
            query_block, jnp.broadcast_to(queries32[s : s + 1], (8, HEADS * KEY)), 0.0
        ).astype(bf16)
        blocked.append(spread_query)
        found = dot_t(spread_query, keys[s])
        distance = jnp.maximum(filled_of(s) - place, 0).astype(f32)
        weights_s[s] = jnp.where(
            place < filled_of(s), found * jnp.exp(distance * rate_wide), 0.0
        ).astype(bf16)

    for g in range(steps):
        for c in group_copies[g]:
            c.wait()
        for s in range(g * GROUP, (g + 1) * GROUP):
            inside = dot(weights_s[s], values[s])
            heads = blocked[s]
            stacked = (
                heads[:, 0:KEY]
                + heads[:, KEY : 2 * KEY]
                + heads[:, 2 * KEY : 3 * KEY]
                + heads[:, 3 * KEY : 4 * KEY]
            )
            carried = jnp.concatenate(
                [dot(stacked, state[s, h].astype(bf16)) for h in range(HEADS)], axis=1
            )
            decay = jnp.exp((filled_of(s).astype(f32) + 1.0) * rate_tall)
            both = jnp.where(value_block, inside + carried * decay, 0.0)
            retained_s[s : s + 1, :] = jnp.sum(both, axis=0, keepdims=True)

    copies[8].wait()
    copies[9].wait()
    new_values = dot(normal_in, wv[...]).astype(bf16)
    new_values_o[...] = new_values
    new_values32 = new_values.astype(f32)
    headed = []
    for h in range(HEADS):
        own = jnp.sum(product[:, h * KEY : (h + 1) * KEY], axis=1, keepdims=True)
        own = own.astype(bf16).astype(f32)
        span = slice(h * VALUE, (h + 1) * VALUE)
        headed.append(normed(retained_s[:, span] + own * new_values32[:, span]).astype(bf16))
    copies[10].wait()
    mixer_out = dot(jnp.concatenate(headed, axis=1), wo[...])
    residual = widened + normed(mixer_out)
    residual_o[...] = residual
    normal_ffn = (normed(residual) * ffn_gain[...]).astype(bf16)
    ffn_o[...] = normal_ffn
    row = jnp.concatenate([normal_ffn, route_weight], axis=1)
    outgoing_o[...] = jnp.broadcast_to(row[None], outgoing_o.shape)
    for c in shard_copies:
        c.wait()


def mixer(
    tokens, lengths, mix_gain, ffn_gain, routes, scores, cache_keys, cache_values, state, wq, wk, wv, wo, gate, up, down
):
    shapes = [
        jax.ShapeDtypeStruct((SEQ, WIDTH), f32),
        jax.ShapeDtypeStruct((SEQ, WIDTH), bf16),
        jax.ShapeDtypeStruct((SEQ, HEADS * KEY), bf16),
        jax.ShapeDtypeStruct((SEQ, WIDTH), bf16),
        jax.ShapeDtypeStruct((NEAR, SEQ, WIDTH + EXPERTS), bf16),
        jax.ShapeDtypeStruct((3 * gate.shape[0], WIDTH), bf16),
    ]
    held = (
        routes.T, scores.T, tokens, mix_gain[None], wq, wk, cache_keys, wv, ffn_gain[None], wo, cache_values, state
    )
    return pl.pallas_call(
        mixer_kernel,
        name="mixer",
        out_shape=shapes,
        in_specs=[hbm] * 16,
        out_specs=[vmem] * 5 + [hbm],
        scratch_shapes=[pltpu.SMEM((SEQ,), jnp.int32)]
        + [pltpu.VMEM(a.shape, a.dtype) for a in held]
        + [
            pltpu.VMEM((SEQ, 8, BLOCK), bf16),
            pltpu.VMEM((SEQ, WIDTH), f32),
            pltpu.SemaphoreType.DMA((11,)),
            pltpu.SemaphoreType.DMA((2, SEQ // GROUP)),
            pltpu.SemaphoreType.DMA((3,)),
        ],
        cost_estimate=pl.CostEstimate(flops=2_000_000_000, bytes_accessed=22_000_000, transcendentals=0),
        compiler_params=pltpu.CompilerParams(vmem_limit_bytes=60 * MIB),
    )(lengths, *held, gate, up, down)


def swiglu(inputs, w_gate, w_up, w_down):
    hidden = (silu(dot(inputs, w_gate)) * dot(inputs, w_up)).astype(bf16)
    return dot(hidden, w_down)


def mixed(bits, masks):
    total = jnp.zeros_like(bits)
    for i, mask in enumerate(masks):
        total = total | (((bits >> i) & 1) * mask)
    return total


def select_kernel(index, near, outgoing_o, combine_o):
    tokens = near[:, :, 0:WIDTH].reshape(NEAR * SEQ, WIDTH)
    weights = near[:, :, WIDTH:].reshape(NEAR * SEQ, EXPERTS)
    expert = mixed(iota((EXPERTS, ROWS), 1) // HELD, far_masks) ^ index[0]
    pick = (iota((EXPERTS, ROWS), 0) == expert).astype(bf16)
    weight = dot(weights, pick)
    named = (weight > 0.0).astype(bf16)
    shape = (NEAR * SEQ, NEAR * SEQ)
    earlier = (iota(shape, 1) < iota(shape, 0)).astype(bf16)
    rank = dot(earlier, named)
    slot = (iota((NEAR * SEQ, ROWS), 1) % HELD).astype(f32)
    combine = jnp.where(rank == slot, weight, 0.0)
    combine_o[...] = combine.astype(bf16)
    chosen = dot_0((combine > 0.0).astype(bf16), tokens).astype(bf16)
    outgoing_o[...] = chosen.reshape(FAR, HELD, WIDTH)


def select(index, near):
    return pl.pallas_call(
        select_kernel,
        name="select",
        out_shape=[
            jax.ShapeDtypeStruct((FAR, HELD, WIDTH), bf16),
            jax.ShapeDtypeStruct((NEAR * SEQ, ROWS), bf16),
        ],
        in_specs=[pl.BlockSpec(memory_space=pltpu.SMEM), vmem],
        out_specs=[vmem] * 2,
        compiler_params=pltpu.CompilerParams(vmem_limit_bytes=8 * MIB),
    )(index, near)


def swiglu(inputs, w_gate, w_up, w_down):
    hidden = (silu(dot(inputs, w_gate)) * dot(inputs, w_up)).astype(bf16)
    return dot(hidden, w_down)


def expert_kernel(arrived, gate, up, down, back):
    rows = arrived[...].reshape(ROWS, WIDTH)
    out = swiglu(rows, gate[0], up[0], down[0]).astype(bf16)
    back[...] = out.reshape(FAR, HELD, WIDTH)


def experts(arrived, gate, up, down):
    return pl.pallas_call(
        expert_kernel,
        name="experts",
        out_shape=jax.ShapeDtypeStruct(arrived.shape, bf16),
        in_specs=[vmem] * 4,
        out_specs=vmem,
        cost_estimate=pl.CostEstimate(flops=500_000_000, bytes_accessed=3_000_000, transcendentals=0),
        compiler_params=pltpu.CompilerParams(vmem_limit_bytes=8 * MIB),
    )(arrived, gate, up, down)


def offsets(masks):
    found = [0]
    for m in masks:
        found = found + [f ^ m for f in found]
    return found


def dense_kernel(*refs):
    near, other, mix = refs[0:3]
    shards, own_o, other_o = refs[3:11], refs[11], refs[12]
    count = NEAR * SEQ
    inputs = jnp.concatenate(
        [t[:, :, 0:WIDTH].reshape(count, WIDTH) for t in (near, other)], axis=0
    )
    n = shards[0].shape[0] // 3
    gates, ups, downs = [
        jnp.concatenate([w[i * n : (i + 1) * n] for w in shards], axis=0) for i in range(3)
    ]
    hidden = (silu(dot_t(inputs, gates)) * dot_t(inputs, ups)).astype(bf16)
    part = (dot(hidden, downs) / (1.0 + jnp.exp(-mix[...]))).astype(bf16)
    own_o[...] = part[0:count].reshape(NEAR, SEQ, WIDTH)
    other_o[...] = part[count:].reshape(NEAR, SEQ, WIDTH)


def dense(near, other, weights, mix):
    part = jax.ShapeDtypeStruct((NEAR, SEQ, WIDTH), bf16)
    return pl.pallas_call(
        dense_kernel,
        name="dense",
        out_shape=[part] * 2,
        in_specs=[vmem] * 11,
        out_specs=[vmem] * 2,
        cost_estimate=pl.CostEstimate(flops=500_000_000, bytes_accessed=4_000_000, transcendentals=0),
        compiler_params=pltpu.CompilerParams(vmem_limit_bytes=12 * MIB),
    )(near, other, mix[None], *weights)


def combine_kernel(back, combine, own, other, parts_o):
    rows = back[...].reshape(ROWS, WIDTH)
    total = dot(combine[...], rows).reshape(NEAR, SEQ, WIDTH)
    parts_o[...] = (total + own[...].astype(f32) + other[...].astype(f32)).astype(bf16)


def combine_near(back, combine, own, other):
    return pl.pallas_call(
        combine_kernel,
        name="combine",
        out_shape=jax.ShapeDtypeStruct((NEAR, SEQ, WIDTH), bf16),
        in_specs=[vmem] * 4,
        out_specs=vmem,
        compiler_params=pltpu.CompilerParams(vmem_limit_bytes=8 * MIB),
    )(back, combine, own, other)


def shared_kernel(own, s_gate, s_up, s_down, out):
    out[...] = swiglu(own[...], s_gate[...], s_up[...], s_down[...])


def shared(own, s_gate, s_up, s_down):
    return pl.pallas_call(
        shared_kernel,
        name="shared",
        out_shape=jax.ShapeDtypeStruct((SEQ, WIDTH), f32),
        in_specs=[vmem] * 4,
        out_specs=vmem,
        cost_estimate=pl.CostEstimate(flops=900_000_000, bytes_accessed=2_000_000, transcendentals=0),
        compiler_params=pltpu.CompilerParams(vmem_limit_bytes=4 * MIB),
    )(own, s_gate, s_up, s_down)


def final_kernel(parts, residual, extra, out):
    combined = extra[...] + jnp.sum(parts[...].astype(f32), axis=0)
    out[...] = (residual[...] + normed(combined)).astype(bf16)


def final(parts, residual, extra):
    return pl.pallas_call(
        final_kernel,
        name="final",
        out_shape=jax.ShapeDtypeStruct(residual.shape, bf16),
        in_specs=[vmem] * 3,
        out_specs=vmem,
        compiler_params=pltpu.CompilerParams(vmem_limit_bytes=4 * MIB),
    )(parts, residual, extra)


near_groups = [[r ^ f for r in offsets(near_masks)] for f in offsets(far_masks)]
far_groups = [[r ^ f for f in offsets(far_masks)] for r in offsets(near_masks)]


def exchange(values, groups):
    return lax.all_to_all(
        values, "ep", split_axis=0, concat_axis=0, axis_index_groups=groups, tiled=True
    )


def per_device(
    tokens,
    lengths,
    cache_keys,
    cache_values,
    retention_state,
    mix_gain,
    query_weight,
    key_weight,
    value_weight,
    out_weight,
    ffn_gain,
    routes,
    route_scores,
    expert_gate,
    expert_up,
    expert_down,
    shared_gate,
    shared_up,
    shared_down,
    dense_gate,
    dense_up,
    dense_down,
    dense_mix,
):
    residual, normal_ffn, new_keys, new_values, outgoing, shard = mixer(
        tokens,
        lengths,
        mix_gain,
        ffn_gain,
        routes,
        route_scores,
        cache_keys,
        cache_values,
        retention_state,
        query_weight,
        key_weight,
        value_weight,
        out_weight,
        dense_gate,
        dense_up,
        dense_down,
    )
    hop = {}
    for m in (2, 8, 32):
        hop[m] = flip(shard, m)
    for m, k in ((2, 8), (8, 32), (32, 2)):
        hop[m | k] = flip(hop[m], k)
    hop[42] = flip(hop[10], 32)
    weights = [shard] + list(hop.values())

    near = exchange(outgoing, near_groups)
    place = lax.axis_index("ep").astype(jnp.int32)
    index = mixed((place >> 2) & 1 | (place >> 3) & 2 | (place >> 4) & 4, near_masks)
    chosen, combine = select(index[None], near)
    other = flip(near, 1)
    own_part, other_part = dense(near, other, weights, dense_mix)
    arrived = exchange(chosen, far_groups)
    outputs = experts(arrived, expert_gate, expert_up, expert_down)
    back = exchange(outputs, far_groups)
    other_part = flip(other_part, 1)
    parts = combine_near(back, combine, own_part, other_part)
    parts = exchange(parts, near_groups)
    extra = shared(normal_ffn, shared_gate, shared_up, shared_down)
    layer_out = final(parts, residual, extra)
    return (layer_out, new_keys, new_values)


def solution(mesh):
    in_specs = (
        P("ep", None),
        P("ep"),
        P("ep", None, None),
        P("ep", None, None),
        P("ep", None, None, None),
        P(),
        P(),
        P(),
        P(),
        P(),
        P(),
        P("ep", None),
        P("ep", None),
        P("ep", None, None),
        P("ep", None, None),
        P("ep", None, None),
        P(),
        P(),
        P(),
        P("ep", None),
        P("ep", None),
        P("ep", None),
        P(),
    )
    out_specs = (P("ep", None), P("ep", None), P("ep", None))

    return jax.shard_map(
        per_device, mesh=mesh, in_specs=in_specs, out_specs=out_specs, check_vma=False
    )
```

profile of v0, /device:TPU:1, one launch (start us, length us, event | category | flops | bytes accessed | tf_op | source)
XLA Modules:
  0.0 87.0 jit_solution(4371133060533598639)
XLA Ops:
  0.6 9.0 %mixer.1 = (f32[16,1024]{1,0:T(8,128)}, bf16[16,1024]{1,0:T(8,128)(2,1)}, bf16[16,512]{1,0:T(8,128)(2,1)}, bf16[16,1024]{1,0:T(8,128)(2,1)}, bf16[8,16,1152]{2,1,0:T(8,128)(2,1)}, /*index=5*/bf16[96,1024]{1,0:T(8,128)(2,1)}) custom-call(s32[16]{0:T(128)} %lengths_h.1, s32[6,16]{1,0:T(8,128)} %bitcast.7, f32[6,16]{1,0:T(8,128)} %bitcast.8, ...), custom_call_target="tpu_custom_call" | custom-call | flops 2000000000 | bytes 22000000 | tf_op jit(solution)/shard_map/mixer/pallas_call | solution.py:281
  9.6 0.0 copy-start
  9.6 0.0 copy-start.1
  9.7 0.0 copy-start.2
  9.7 10.6 %all-to-all-start = ((bf16[8,16,1152]{2,1,0:T(8,128)(2,1)}), bf16[8,16,1152]{2,1,0:T(8,128)(2,1)S(1)}, u32[]{:S(2)}, u32[]{:S(2)}) async-start(bf16[8,16,1152]{2,1,0:T(8,128)(2,1)} %get-tuple-element.13), calls=%async_computation | async-start | bytes 589824 | tf_op jit(solution)/shard_map/all_to_all | solution.py:458
  20.3 9.8 %all-to-all-done.near.refs_0_ = bf16[8,16,1152]{2,1,0:T(8,128)(2,1)S(1)} async-done(((bf16[8,16,1152]{2,1,0:T(8,128)(2,1)}), bf16[8,16,1152]{2,1,0:T(8,128)(2,1)S(1)}, u32[]{:S(2)}, u32[]{:S(2)}) %all-to-all-start) | async-done | bytes 294944 | tf_op jit(solution)/shard_map/all_to_all | solution.py:458
  30.1 1.4 %select.1 = (bf16[16,16,1024]{2,1,0:T(8,128)(2,1)}, bf16[128,256]{1,0:T(8,128)(2,1)S(1)}) custom-call(s32[1]{0:T(128)} %bitcast.index, bf16[8,16,1152]{2,1,0:T(8,128)(2,1)S(1)} %all-to-all-done.near.refs_0_), custom_call_target="tpu_custom_call" | custom-call | tf_op jit(solution)/shard_map/select/pallas_call | solution.py:331
  31.5 5.5 %all-to-all-start.1 = ((bf16[16,16,1024]{2,1,0:T(8,128)(2,1)}), bf16[16,16,1024]{2,1,0:T(8,128)(2,1)S(1)}, u32[]{:S(2)}, u32[]{:S(2)}) async-start(bf16[16,16,1024]{2,1,0:T(8,128)(2,1)} %get-tuple-element.14), calls=%async_computation.1 | async-start | bytes 1048576 | tf_op jit(solution)/shard_map/all_to_all | solution.py:458
  37.0 0.0 copy-start.3
  37.0 0.0 copy-start.5
  37.0 1.4 %collective-permute-start.1 = (bf16[96,1024]{1,0:T(8,128)(2,1)}, bf16[96,1024]{1,0:T(8,128)(2,1)S(1)}, u32[]{:S(2)}, u32[]{:S(2)}) collective-permute-start(bf16[96,1024]{1,0:T(8,128)(2,1)} %get-tuple-element.16.refs_3_), channel_id=1, source_target_pairs={{0,2},{1,3},{2,0},{3,1},{4,6},{5,7},{6,4},{7,5},{8,10},{9,11},{10,... | collective-permute-start | bytes 589832 | tf_op jit(solution)/shard_map/ppermute | solution.py:40
  38.5 1.2 %collective-permute-start.2 = (bf16[96,1024]{1,0:T(8,128)(2,1)}, bf16[96,1024]{1,0:T(8,128)(2,1)S(1)}, u32[]{:S(2)}, u32[]{:S(2)}) collective-permute-start(bf16[96,1024]{1,0:T(8,128)(2,1)} %get-tuple-element.16.refs_3_), channel_id=1, source_target_pairs={{0,8},{1,9},{2,10},{3,11},{4,12},{5,13},{6,14},{7,15},{8,0},{9,1},... | collective-permute-start | bytes 589832 | tf_op jit(solution)/shard_map/ppermute | solution.py:40
  39.7 1.2 %collective-permute-start.3 = (bf16[96,1024]{1,0:T(8,128)(2,1)}, bf16[96,1024]{1,0:T(8,128)(2,1)S(1)}, u32[]{:S(2)}, u32[]{:S(2)}) collective-permute-start(bf16[96,1024]{1,0:T(8,128)(2,1)} %get-tuple-element.16.refs_3_), channel_id=1, source_target_pairs={{0,32},{1,33},{2,34},{3,35},{4,36},{5,37},{6,38},{7,39},{8,40},{9,... | collective-permute-start | bytes 589832 | tf_op jit(solution)/shard_map/ppermute | solution.py:40
  40.9 8.2 %collective-permute-done.1.refs_4_ = bf16[96,1024]{1,0:T(8,128)(2,1)S(1)} collective-permute-done((bf16[96,1024]{1,0:T(8,128)(2,1)}, bf16[96,1024]{1,0:T(8,128)(2,1)S(1)}, u32[]{:S(2)}, u32[]{:S(2)}) %collective-permute-start.1) | collective-permute-done | bytes 196640 | tf_op jit(solution)/shard_map/ppermute | solution.py:40
  49.1 1.2 %collective-permute-start.4 = (bf16[96,1024]{1,0:T(8,128)(2,1)S(1)}, bf16[96,1024]{1,0:T(8,128)(2,1)}, u32[]{:S(2)}, u32[]{:S(2)}) collective-permute-start(bf16[96,1024]{1,0:T(8,128)(2,1)S(1)} %collective-permute-done.1.refs_4_), channel_id=1, source_target_pairs={{0,8},{1,9},{2,10},{3,11},{4,12},{5,13},{6,14},{7,15},{8,0},{9,1},... | collective-permute-start | bytes 589832 | tf_op jit(solution)/shard_map/ppermute | solution.py:40
  50.3 1.2 %collective-permute-start = (bf16[8,16,1152]{2,1,0:T(8,128)(2,1)S(1)}, bf16[8,16,1152]{2,1,0:T(8,128)(2,1)S(1)}, u32[]{:S(2)}, u32[]{:S(2)}) collective-permute-start(bf16[8,16,1152]{2,1,0:T(8,128)(2,1)S(1)} %all-to-all-done.near.refs_0_), channel_id=1, source_target_pairs={{0,1},{1,0},{2,3},{3,2},{4,5},{5,4},{6,7},{7,6},{8,9},{9,8},{10,11... | collective-permute-start | bytes 884744 | tf_op jit(solution)/shard_map/ppermute | solution.py:40
  51.5 0.0 collective-permute-done.2.refs_5_
  51.5 1.2 %collective-permute-start.5 = (bf16[96,1024]{1,0:T(8,128)(2,1)S(1)}, bf16[96,1024]{1,0:T(8,128)(2,1)}, u32[]{:S(2)}, u32[]{:S(2)}) collective-permute-start(bf16[96,1024]{1,0:T(8,128)(2,1)S(1)} %collective-permute-done.2.refs_5_), channel_id=1, source_target_pairs={{0,32},{1,33},{2,34},{3,35},{4,36},{5,37},{6,38},{7,39},{8,40},{9,... | collective-permute-start | bytes 589832 | tf_op jit(solution)/shard_map/ppermute | solution.py:40
  52.8 0.0 collective-permute-done.3.refs_6_
  52.8 0.3 collective-permute-start.6
  53.1 1.6 %collective-permute-done.4.refs_7_ = bf16[96,1024]{1,0:T(8,128)(2,1)} collective-permute-done((bf16[96,1024]{1,0:T(8,128)(2,1)S(1)}, bf16[96,1024]{1,0:T(8,128)(2,1)}, u32[]{:S(2)}, u32[]{:S(2)}) %collective-permute-start.4) | collective-permute-done | bytes 196640 | tf_op jit(solution)/shard_map/ppermute | solution.py:40
  54.7 1.2 %collective-permute-start.7 = (bf16[96,1024]{1,0:T(8,128)(2,1)}, bf16[96,1024]{1,0:T(8,128)(2,1)}, u32[]{:S(2)}, u32[]{:S(2)}) collective-permute-start(bf16[96,1024]{1,0:T(8,128)(2,1)} %collective-permute-done.4.refs_7_), channel_id=1, source_target_pairs={{0,32},{1,33},{2,34},{3,35},{4,36},{5,37},{6,38},{7,39},{8,40},{9,... | collective-permute-start | bytes 589832 | tf_op jit(solution)/shard_map/ppermute | solution.py:40
  55.9 0.0 all-to-all-done.1.arrived
  55.9 0.0 copy-done
  55.9 0.0 copy-done.1
  55.9 0.0 copy-done.2
  55.9 1.5 %experts.1 = bf16[16,16,1024]{2,1,0:T(8,128)(2,1)} custom-call(bf16[16,16,1024]{2,1,0:T(8,128)(2,1)S(1)} %all-to-all-done.1.arrived, bf16[1,1024,256]{2,1,0:T(8,128)(2,1)S(1)} %copy-done, bf16[1,1024,256]{2,1,0:T(8,128)(2,1)S(1)} %copy-done.1, bf16[1,256,1024]{2,1,0:T(8,128)(2,1)S(1)} %copy-done.2), custom_call_target="tpu_custom_call" | custom-call | flops 500000000 | bytes 3000000 | tf_op jit(solution)/shard_map/experts/pallas_call | solution.py:356
  57.4 5.5 %all-to-all-start.2 = ((bf16[16,16,1024]{2,1,0:T(8,128)(2,1)}), bf16[16,16,1024]{2,1,0:T(8,128)(2,1)S(1)}, u32[]{:S(2)}, u32[]{:S(2)}) async-start(bf16[16,16,1024]{2,1,0:T(8,128)(2,1)} %experts.1), calls=%async_computation.2 | async-start | bytes 1048576 | tf_op jit(solution)/shard_map/all_to_all | solution.py:458
  62.9 0.0 copy-start.6
  62.9 0.0 copy-start.7
  62.9 0.0 collective-permute-done.5.refs_8_
  62.9 0.0 collective-permute-done.6.refs_9_
  63.0 0.0 collective-permute-done.refs_1_
  63.0 0.0 collective-permute-done.7.refs_10_
  63.0 0.0 copy-done.3
  63.0 0.0 copy-done.5
  63.0 2.0 %dense.1 = (bf16[8,16,1024]{2,1,0:T(8,128)(2,1)S(1)}, bf16[8,16,1024]{2,1,0:T(8,128)(2,1)S(1)}) custom-call(bf16[8,16,1152]{2,1,0:T(8,128)(2,1)S(1)} %all-to-all-done.near.refs_0_, bf16[8,16,1152]{2,1,0:T(8,128)(2,1)S(1)} %collective-permute-done.refs_1_, f32[1,1024]{1,0:T(1,128)S(1)} %bitcast.6, bf16[96,1024]{1,0:T(8,128)(2,1)S(1)} %copy-done.3, ...), custom_call_target="tpu_custom_call" | custom-call | flops 500000000 | bytes 4000000 | tf_op jit(solution)/shard_map/dense/pallas_call | solution.py:393
  65.0 0.3 collective-permute-start.8
  65.3 1.3 %collective-permute-done.8.other = bf16[8,16,1024]{2,1,0:T(8,128)(2,1)S(1)} collective-permute-done((bf16[8,16,1024]{2,1,0:T(8,128)(2,1)S(1)}, bf16[8,16,1024]{2,1,0:T(8,128)(2,1)S(1)}, u32[]{:S(2)}, u32[]{:S(2)}) %collective-permute-start.8) | collective-permute-done | bytes 262176 | tf_op jit(solution)/shard_map/ppermute | solution.py:40
  66.6 5.8 %all-to-all-done.2.back = bf16[16,16,1024]{2,1,0:T(8,128)(2,1)S(1)} async-done(((bf16[16,16,1024]{2,1,0:T(8,128)(2,1)}), bf16[16,16,1024]{2,1,0:T(8,128)(2,1)S(1)}, u32[]{:S(2)}, u32[]{:S(2)}) %all-to-all-start.2) | async-done | bytes 524320 | tf_op jit(solution)/shard_map/all_to_all | solution.py:458
  72.4 0.9 %combine.1 = bf16[8,16,1024]{2,1,0:T(8,128)(2,1)} custom-call(bf16[16,16,1024]{2,1,0:T(8,128)(2,1)S(1)} %all-to-all-done.2.back, bf16[128,256]{1,0:T(8,128)(2,1)S(1)} %get-tuple-element.15.combine, bf16[8,16,1024]{2,1,0:T(8,128)(2,1)S(1)} %get-tuple-element.17.own, bf16[8,16,1024]{2,1,0:T(8,128)(2,1)S(1)} %collective-permute-done.8.other), custom_call_target="tpu_custom_call" | custom-call | tf_op jit(solution)/shard_map/combine/pallas_call | solution.py:411
  73.3 0.0 copy-start.4
  73.3 3.5 %all-to-all-start.3 = ((bf16[8,16,1024]{2,1,0:T(8,128)(2,1)}), bf16[8,16,1024]{2,1,0:T(8,128)(2,1)S(1)}, u32[]{:S(2)}, u32[]{:S(2)}) async-start(bf16[8,16,1024]{2,1,0:T(8,128)(2,1)} %combine.1), calls=%async_computation.3 | async-start | bytes 524288 | tf_op jit(solution)/shard_map/all_to_all | solution.py:458
  76.9 0.0 copy-done.6
  76.9 0.0 copy-done.7
  76.9 0.0 copy-start.8
  76.9 1.0 %copy-done.8 = bf16[256,1024]{1,0:T(8,128)(2,1)S(1)} copy-done((bf16[256,1024]{1,0:T(8,128)(2,1)S(1)}, bf16[256,1024]{1,0:T(8,128)(2,1)}, u32[]{:S(2)}) %copy-start.8) | copy-done | bytes 524312
  77.9 0.0 copy-start.9
  77.9 0.8 copy-done.9
  78.7 0.4 shared.1.extra
  79.1 7.2 %all-to-all-done.3.parts = bf16[8,16,1024]{2,1,0:T(8,128)(2,1)S(1)} async-done(((bf16[8,16,1024]{2,1,0:T(8,128)(2,1)}), bf16[8,16,1024]{2,1,0:T(8,128)(2,1)S(1)}, u32[]{:S(2)}, u32[]{:S(2)}) %all-to-all-start.3) | async-done | bytes 262176 | tf_op jit(solution)/shard_map/all_to_all | solution.py:458
  86.2 0.0 copy-done.4
  86.2 0.7 final.1
Async XLA Ops:
  9.6 46.3 %copy-start = (bf16[1,1024,256]{2,1,0:T(8,128)(2,1)S(1)}, bf16[1,1024,256]{2,1,0:T(8,128)(2,1)}, u32[]{:S(2)}) copy-start(bf16[1,1024,256]{2,1,0:T(8,128)(2,1)} %gate.1) | copy-start | bytes 1572868
  9.6 46.3 %copy-start.1 = (bf16[1,1024,256]{2,1,0:T(8,128)(2,1)S(1)}, bf16[1,1024,256]{2,1,0:T(8,128)(2,1)}, u32[]{:S(2)}) copy-start(bf16[1,1024,256]{2,1,0:T(8,128)(2,1)} %up.1) | copy-start | bytes 1572868
  9.7 46.3 %copy-start.2 = (bf16[1,256,1024]{2,1,0:T(8,128)(2,1)S(1)}, bf16[1,256,1024]{2,1,0:T(8,128)(2,1)}, u32[]{:S(2)}) copy-start(bf16[1,256,1024]{2,1,0:T(8,128)(2,1)} %down.1) | copy-start | bytes 1572868
  9.7 20.4 %all-to-all-start = ((bf16[8,16,1152]{2,1,0:T(8,128)(2,1)}), bf16[8,16,1152]{2,1,0:T(8,128)(2,1)S(1)}, u32[]{:S(2)}, u32[]{:S(2)}) async-start(bf16[8,16,1152]{2,1,0:T(8,128)(2,1)} %get-tuple-element.13), calls=%async_computation | async-start | bytes 589824 | tf_op jit(solution)/shard_map/all_to_all | solution.py:458
  31.5 24.4 %all-to-all-start.1 = ((bf16[16,16,1024]{2,1,0:T(8,128)(2,1)}), bf16[16,16,1024]{2,1,0:T(8,128)(2,1)S(1)}, u32[]{:S(2)}, u32[]{:S(2)}) async-start(bf16[16,16,1024]{2,1,0:T(8,128)(2,1)} %get-tuple-element.14), calls=%async_computation.1 | async-start | bytes 1048576 | tf_op jit(solution)/shard_map/all_to_all | solution.py:458
  37.0 26.0 %copy-start.3 = (bf16[96,1024]{1,0:T(8,128)(2,1)S(1)}, bf16[96,1024]{1,0:T(8,128)(2,1)}, u32[]{:S(2)}) copy-start(bf16[96,1024]{1,0:T(8,128)(2,1)} %get-tuple-element.16.refs_3_) | copy-start | bytes 589828
  37.0 26.0 %copy-start.5 = (f32[1024]{0:T(1024)S(1)}, f32[1024]{0:T(1024)}, u32[]{:S(2)}) copy-start(f32[1024]{0:T(1024)} %param.45) | copy-start | bytes 12292
  37.0 12.1 %collective-permute-start.1 = (bf16[96,1024]{1,0:T(8,128)(2,1)}, bf16[96,1024]{1,0:T(8,128)(2,1)S(1)}, u32[]{:S(2)}, u32[]{:S(2)}) collective-permute-start(bf16[96,1024]{1,0:T(8,128)(2,1)} %get-tuple-element.16.refs_3_), channel_id=1, source_target_pairs={{0,2},{1,3},{2,0},{3,1},{4,6},{5,7},{6,4},{7,5},{8,10},{9,11},{10,... | collective-permute-start | bytes 589832 | tf_op jit(solution)/shard_map/ppermute | solution.py:40
  38.5 13.1 %collective-permute-start.2 = (bf16[96,1024]{1,0:T(8,128)(2,1)}, bf16[96,1024]{1,0:T(8,128)(2,1)S(1)}, u32[]{:S(2)}, u32[]{:S(2)}) collective-permute-start(bf16[96,1024]{1,0:T(8,128)(2,1)} %get-tuple-element.16.refs_3_), channel_id=1, source_target_pairs={{0,8},{1,9},{2,10},{3,11},{4,12},{5,13},{6,14},{7,15},{8,0},{9,1},... | collective-permute-start | bytes 589832 | tf_op jit(solution)/shard_map/ppermute | solution.py:40
  39.7 13.1 %collective-permute-start.3 = (bf16[96,1024]{1,0:T(8,128)(2,1)}, bf16[96,1024]{1,0:T(8,128)(2,1)S(1)}, u32[]{:S(2)}, u32[]{:S(2)}) collective-permute-start(bf16[96,1024]{1,0:T(8,128)(2,1)} %get-tuple-element.16.refs_3_), channel_id=1, source_target_pairs={{0,32},{1,33},{2,34},{3,35},{4,36},{5,37},{6,38},{7,39},{8,40},{9,... | collective-permute-start | bytes 589832 | tf_op jit(solution)/shard_map/ppermute | solution.py:40
  49.1 5.6 %collective-permute-start.4 = (bf16[96,1024]{1,0:T(8,128)(2,1)S(1)}, bf16[96,1024]{1,0:T(8,128)(2,1)}, u32[]{:S(2)}, u32[]{:S(2)}) collective-permute-start(bf16[96,1024]{1,0:T(8,128)(2,1)S(1)} %collective-permute-done.1.refs_4_), channel_id=1, source_target_pairs={{0,8},{1,9},{2,10},{3,11},{4,12},{5,13},{6,14},{7,15},{8,0},{9,1},... | collective-permute-start | bytes 589832 | tf_op jit(solution)/shard_map/ppermute | solution.py:40
  50.3 12.7 %collective-permute-start = (bf16[8,16,1152]{2,1,0:T(8,128)(2,1)S(1)}, bf16[8,16,1152]{2,1,0:T(8,128)(2,1)S(1)}, u32[]{:S(2)}, u32[]{:S(2)}) collective-permute-start(bf16[8,16,1152]{2,1,0:T(8,128)(2,1)S(1)} %all-to-all-done.near.refs_0_), channel_id=1, source_target_pairs={{0,1},{1,0},{2,3},{3,2},{4,5},{5,4},{6,7},{7,6},{8,9},{9,8},{10,11... | collective-permute-start | bytes 884744 | tf_op jit(solution)/shard_map/ppermute | solution.py:40
  51.5 11.4 %collective-permute-start.5 = (bf16[96,1024]{1,0:T(8,128)(2,1)S(1)}, bf16[96,1024]{1,0:T(8,128)(2,1)}, u32[]{:S(2)}, u32[]{:S(2)}) collective-permute-start(bf16[96,1024]{1,0:T(8,128)(2,1)S(1)} %collective-permute-done.2.refs_5_), channel_id=1, source_target_pairs={{0,32},{1,33},{2,34},{3,35},{4,36},{5,37},{6,38},{7,39},{8,40},{9,... | collective-permute-start | bytes 589832 | tf_op jit(solution)/shard_map/ppermute | solution.py:40
  52.8 10.2 %collective-permute-start.6 = (bf16[96,1024]{1,0:T(8,128)(2,1)S(1)}, bf16[96,1024]{1,0:T(8,128)(2,1)}, u32[]{:S(2)}, u32[]{:S(2)}) collective-permute-start(bf16[96,1024]{1,0:T(8,128)(2,1)S(1)} %collective-permute-done.3.refs_6_), channel_id=1, source_target_pairs={{0,2},{1,3},{2,0},{3,1},{4,6},{5,7},{6,4},{7,5},{8,10},{9,11},{10,... | collective-permute-start | bytes 589832 | tf_op jit(solution)/shard_map/ppermute | solution.py:40
  54.7 8.3 %collective-permute-start.7 = (bf16[96,1024]{1,0:T(8,128)(2,1)}, bf16[96,1024]{1,0:T(8,128)(2,1)}, u32[]{:S(2)}, u32[]{:S(2)}) collective-permute-start(bf16[96,1024]{1,0:T(8,128)(2,1)} %collective-permute-done.4.refs_7_), channel_id=1, source_target_pairs={{0,32},{1,33},{2,34},{3,35},{4,36},{5,37},{6,38},{7,39},{8,40},{9,... | collective-permute-start | bytes 589832 | tf_op jit(solution)/shard_map/ppermute | solution.py:40
  57.4 14.9 %all-to-all-start.2 = ((bf16[16,16,1024]{2,1,0:T(8,128)(2,1)}), bf16[16,16,1024]{2,1,0:T(8,128)(2,1)S(1)}, u32[]{:S(2)}, u32[]{:S(2)}) async-start(bf16[16,16,1024]{2,1,0:T(8,128)(2,1)} %experts.1), calls=%async_computation.2 | async-start | bytes 1048576 | tf_op jit(solution)/shard_map/all_to_all | solution.py:458
  62.9 13.9 %copy-start.6 = (bf16[1024,256]{1,0:T(8,128)(2,1)S(1)}, bf16[1024,256]{1,0:T(8,128)(2,1)}, u32[]{:S(2)}) copy-start(bf16[1024,256]{1,0:T(8,128)(2,1)} %s_gate.1) | copy-start | bytes 1572868
  62.9 13.9 %copy-start.7 = (bf16[1024,256]{1,0:T(8,128)(2,1)S(1)}, bf16[1024,256]{1,0:T(8,128)(2,1)}, u32[]{:S(2)}) copy-start(bf16[1024,256]{1,0:T(8,128)(2,1)} %s_up.1) | copy-start | bytes 1572868
  65.0 1.6 %collective-permute-start.8 = (bf16[8,16,1024]{2,1,0:T(8,128)(2,1)S(1)}, bf16[8,16,1024]{2,1,0:T(8,128)(2,1)S(1)}, u32[]{:S(2)}, u32[]{:S(2)}) collective-permute-start(bf16[8,16,1024]{2,1,0:T(8,128)(2,1)S(1)} %get-tuple-element.18), channel_id=1, source_target_pairs={{0,1},{1,0},{2,3},{3,2},{4,5},{5,4},{6,7},{7,6},{8,9},{9,8},{10,11... | collective-permute-start | bytes 786440 | tf_op jit(solution)/shard_map/ppermute | solution.py:40
  73.3 12.9 %copy-start.4 = (f32[16,1024]{1,0:T(8,128)S(1)}, f32[16,1024]{1,0:T(8,128)}, u32[]{:S(2)}) copy-start(f32[16,1024]{1,0:T(8,128)} %get-tuple-element.19.residual) | copy-start | bytes 196612
  73.3 12.9 %all-to-all-start.3 = ((bf16[8,16,1024]{2,1,0:T(8,128)(2,1)}), bf16[8,16,1024]{2,1,0:T(8,128)(2,1)S(1)}, u32[]{:S(2)}, u32[]{:S(2)}) async-start(bf16[8,16,1024]{2,1,0:T(8,128)(2,1)} %combine.1), calls=%async_computation.3 | async-start | bytes 524288 | tf_op jit(solution)/shard_map/all_to_all | solution.py:458
  76.9 1.0 %copy-start.8 = (bf16[256,1024]{1,0:T(8,128)(2,1)S(1)}, bf16[256,1024]{1,0:T(8,128)(2,1)}, u32[]{:S(2)}) copy-start(bf16[256,1024]{1,0:T(8,128)(2,1)} %s_down.1) | copy-start | bytes 1572868
  77.9 0.8 copy-start.9
where the time goes:
time: 88.7 us; the launch traced here: 87 us
  starting transfers between devices  34.5 us (39%)
  waiting for transfers between devices  33.8 us (38%)
  Pallas kernels  16 us (18%)
  local copies, waits for them, and re-layouts  1.84 us (2%)
    all_to_all x4, starting transfers between devices, exchange(): lax.all_to_all(values, 'ep', split_axis=0, concat_axis=0, axis_index_grou...  25.1 us
    all_to_all x4, waiting for transfers between devices, exchange(): lax.all_to_all(values, 'ep', split_axis=0, concat_axis=0, axis_index_grou...  22.7 us
    ppermute x9, waiting for transfers between devices, flip(): lax.ppermute(values, 'ep', [(i, i ^ mask) for i in range(lax.axis_size('e...  11.1 us
    ppermute x9, starting transfers between devices, flip(): lax.ppermute(values, 'ep', [(i, i ^ mask) for i in range(lax.axis_size('e...  9.4 us
    pallas_call x1, Pallas kernels, mixer(): pl.pallas_call(mixer_kernel, name='mixer', out_shape=shapes, in_specs=[hb...  8.99 us
    pallas_call x1, Pallas kernels, dense(): pl.pallas_call(dense_kernel, name='dense', out_shape=[part] * 2, in_specs...  1.99 us
    unnamed x20, local copies, waits for them, and re-layouts  1.84 us
  transfers between devices with their start and end apart: 13, of which 6 were waited for; matrix products, arithmetic and copies ran while one was open for 0% of the time, Pallas kernels for 4%

commit v1 on v0

--- a/solution.py
+++ b/solution.py
@@ -27,8 +27,10 @@
 GROUP = 4
 MIB = 1024 * 1024
 
-near_masks = (6, 24, 96)
-far_masks = (1, 2, 8, 32)
+near_masks = (1, 2, 4)
+far_masks = (8, 16, 32, 64)
+wide_mask = 8
+weight_masks = (32, 96, 24)
 
 f32 = jnp.float32
 bf16 = jnp.bfloat16
@@ -401,21 +403,51 @@
     )(near, other, mix[None], *weights)
 
 
-def combine_kernel(back, combine, own, other, parts_o):
+def combine_kernel(place, back, combine, own, other, keep_o, send_o, total_s):
     rows = back[...].reshape(ROWS, WIDTH)
     total = dot(combine[...], rows).reshape(NEAR, SEQ, WIDTH)
-    parts_o[...] = (total + own[...].astype(f32) + other[...].astype(f32)).astype(bf16)
-
-
-def combine_near(back, combine, own, other):
+    total_s[...] = total + own[...].astype(f32) + other[...].astype(f32)
+    for j, k in enumerate((0, 6, 2, 4)):
+        span = slice(j * SEQ, (j + 1) * SEQ)
+        keep_o[span] = total_s[place[0] ^ k]
+        send_o[span] = total_s[place[0] ^ (k + 1)].astype(bf16)
+
+
+def halves(rows):
+    return [
+        jax.ShapeDtypeStruct((rows // 2, WIDTH), f32),
+        jax.ShapeDtypeStruct((rows // 2, WIDTH), bf16),
+    ]
+
+
+def combine_near(place, back, combine, own, other):
     return pl.pallas_call(
         combine_kernel,
         name="combine",
-        out_shape=jax.ShapeDtypeStruct((NEAR, SEQ, WIDTH), bf16),
-        in_specs=[vmem] * 4,
-        out_specs=vmem,
+        out_shape=halves(NEAR * SEQ),
+        in_specs=[pl.BlockSpec(memory_space=pltpu.SMEM)] + [vmem] * 4,
+        out_specs=[vmem] * 2,
+        scratch_shapes=[pltpu.VMEM((NEAR, SEQ, WIDTH), f32)],
         compiler_params=pltpu.CompilerParams(vmem_limit_bytes=8 * MIB),
-    )(back, combine, own, other)
+    )(place, back, combine, own, other)
+
+
+def fold_kernel(kept, came, keep_o, send_o):
+    total = kept[...] + came[...].astype(f32)
+    half = total.shape[0] // 2
+    keep_o[...] = total[0:half]
+    send_o[...] = total[half:].astype(bf16)
+
+
+def fold(kept, came):
+    return pl.pallas_call(
+        fold_kernel,
+        name="fold",
+        out_shape=halves(kept.shape[0]),
+        in_specs=[vmem] * 2,
+        out_specs=[vmem] * 2,
+        compiler_params=pltpu.CompilerParams(vmem_limit_bytes=2 * MIB),
+    )(kept, came)
 
 
 def shared_kernel(own, s_gate, s_up, s_down, out):
@@ -434,20 +466,20 @@
     )(own, s_gate, s_up, s_down)
 
 
-def final_kernel(parts, residual, extra, out):
-    combined = extra[...] + jnp.sum(parts[...].astype(f32), axis=0)
+def final_kernel(kept, came, residual, extra, out):
+    combined = extra[...] + kept[...] + came[...].astype(f32)
     out[...] = (residual[...] + normed(combined)).astype(bf16)
 
 
-def final(parts, residual, extra):
+def final(kept, came, residual, extra):
     return pl.pallas_call(
         final_kernel,
         name="final",
         out_shape=jax.ShapeDtypeStruct(residual.shape, bf16),
-        in_specs=[vmem] * 3,
+        in_specs=[vmem] * 4,
         out_specs=vmem,
         compiler_params=pltpu.CompilerParams(vmem_limit_bytes=4 * MIB),
-    )(parts, residual, extra)
+    )(kept, came, residual, extra)
 
 
 near_groups = [[r ^ f for r in offsets(near_masks)] for f in offsets(far_masks)]
@@ -504,27 +536,31 @@
         dense_down,
     )
     hop = {}
-    for m in (2, 8, 32):
+    for m in weight_masks:
         hop[m] = flip(shard, m)
-    for m, k in ((2, 8), (8, 32), (32, 2)):
-        hop[m | k] = flip(hop[m], k)
-    hop[42] = flip(hop[10], 32)
+    first, second, third = weight_masks
+    for m, k in ((first, second), (second, third), (third, first)):
+        hop[m ^ k] = flip(hop[m], k)
+    hop[first ^ second ^ third] = flip(hop[first ^ second], third)
     weights = [shard] + list(hop.values())
 
     near = exchange(outgoing, near_groups)
     place = lax.axis_index("ep").astype(jnp.int32)
-    index = mixed((place >> 2) & 1 | (place >> 3) & 2 | (place >> 4) & 4, near_masks)
+    index = place & 7
     chosen, combine = select(index[None], near)
-    other = flip(near, 1)
+    other = flip(near, wide_mask)
     own_part, other_part = dense(near, other, weights, dense_mix)
     arrived = exchange(chosen, far_groups)
     outputs = experts(arrived, expert_gate, expert_up, expert_down)
     back = exchange(outputs, far_groups)
-    other_part = flip(other_part, 1)
-    parts = combine_near(back, combine, own_part, other_part)
-    parts = exchange(parts, near_groups)
+    other_part = flip(other_part, wide_mask)
+    kept, sent = combine_near(index[None], back, combine, own_part, other_part)
+    for m in (1, 2):
+        came = flip(sent, m)
+        kept, sent = fold(kept, came)
+    came = flip(sent, 6)
     extra = shared(normal_ffn, shared_gate, shared_up, shared_down)
-    layer_out = final(parts, residual, extra)
+    layer_out = final(kept, came, residual, extra)
     return (layer_out, new_keys, new_values)
 
 

time: 88.7 us -> 84.3 us (0.950)
  the two profiles are of different devices: /device:TPU:1 before, /device:TPU:0 now
where the time goes in v1:
time: 84.3 us; the launch traced here: 83.7 us
  starting transfers between devices  36.6 us (43%)
  waiting for transfers between devices  29.2 us (35%)
  Pallas kernels  15.3 us (18%)
  local copies, waits for them, and re-layouts  1.85 us (2%)
    ppermute x12, waiting for transfers between devices, flip(): lax.ppermute(values, 'ep', [(i, i ^ mask) for i in range(lax.axis_size('e...  20.5 us
    ppermute x12, starting transfers between devices, flip(): lax.ppermute(values, 'ep', [(i, i ^ mask) for i in range(lax.axis_size('e...  19.8 us
    all_to_all x3, starting transfers between devices, exchange(): lax.all_to_all(values, 'ep', split_axis=0, concat_axis=0, axis_index_grou...  16.8 us
    pallas_call x1, Pallas kernels, mixer(): pl.pallas_call(mixer_kernel, name='mixer', out_shape=shapes, in_specs=[hb...  8.98 us
    all_to_all x3, waiting for transfers between devices, exchange(): lax.all_to_all(values, 'ep', split_axis=0, concat_axis=0, axis_index_grou...  8.67 us
    pallas_call x1, Pallas kernels, dense(): pl.pallas_call(dense_kernel, name='dense', out_shape=[part] * 2, in_specs...  1.99 us
    unnamed x20, local copies, waits for them, and re-layouts  1.85 us
  transfers between devices with their start and end apart: 15, of which 8 were waited for; matrix products, arithmetic and copies ran while one was open for 0% of the time, Pallas kernels for 5%

profile of v1, /device:TPU:0, one launch (start us, length us, event | category | flops | bytes accessed | tf_op | source)
XLA Modules:
  0.0 83.7 jit_solution(1680203125536089589)
XLA Ops:
  0.6 9.0 %mixer.1 = (f32[16,1024]{1,0:T(8,128)}, bf16[16,1024]{1,0:T(8,128)(2,1)}, bf16[16,512]{1,0:T(8,128)(2,1)}, bf16[16,1024]{1,0:T(8,128)(2,1)}, bf16[8,16,1152]{2,1,0:T(8,128)(2,1)}, /*index=5*/bf16[96,1024]{1,0:T(8,128)(2,1)}) custom-call(s32[16]{0:T(128)} %lengths_h.1, s32[6,16]{1,0:T(8,128)} %bitcast.7, f32[6,16]{1,0:T(8,128)} %bitcast.8, ...), custom_call_target="tpu_custom_call" | custom-call | flops 2000000000 | bytes 22000000 | tf_op jit(solution)/shard_map/mixer/pallas_call | solution.py:283
  9.6 0.0 copy-start
  9.6 0.0 copy-start.1
  9.6 0.0 copy-start.2
  9.7 4.6 %all-to-all-start = ((bf16[8,16,1152]{2,1,0:T(8,128)(2,1)}), bf16[8,16,1152]{2,1,0:T(8,128)(2,1)S(1)}, u32[]{:S(2)}, u32[]{:S(2)}) async-start(bf16[8,16,1152]{2,1,0:T(8,128)(2,1)} %get-tuple-element.19), calls=%async_computation | async-start | bytes 589824 | tf_op jit(solution)/shard_map/all_to_all | solution.py:490
  14.2 7.9 %all-to-all-done.near.refs_0_ = bf16[8,16,1152]{2,1,0:T(8,128)(2,1)S(1)} async-done(((bf16[8,16,1152]{2,1,0:T(8,128)(2,1)}), bf16[8,16,1152]{2,1,0:T(8,128)(2,1)S(1)}, u32[]{:S(2)}, u32[]{:S(2)}) %all-to-all-start) | async-done | bytes 294944 | tf_op jit(solution)/shard_map/all_to_all | solution.py:490
  22.1 1.4 %select.1 = (bf16[16,16,1024]{2,1,0:T(8,128)(2,1)}, bf16[128,256]{1,0:T(8,128)(2,1)S(1)}) custom-call(s32[1]{0:T(128)} %bitcast.index.place, bf16[8,16,1152]{2,1,0:T(8,128)(2,1)S(1)} %all-to-all-done.near.refs_0_), custom_call_target="tpu_custom_call" | custom-call | tf_op jit(solution)/shard_map/select/pallas_call | solution.py:333
  23.5 8.0 %all-to-all-start.1 = ((bf16[16,16,1024]{2,1,0:T(8,128)(2,1)}), bf16[16,16,1024]{2,1,0:T(8,128)(2,1)S(1)}, u32[]{:S(2)}, u32[]{:S(2)}) async-start(bf16[16,16,1024]{2,1,0:T(8,128)(2,1)} %get-tuple-element.20), calls=%async_computation.1 | async-start | bytes 1048576 | tf_op jit(solution)/shard_map/all_to_all | solution.py:490
  31.6 0.0 copy-start.3
  31.6 0.0 copy-start.5
  31.6 2.0 %collective-permute-start.1 = (bf16[96,1024]{1,0:T(8,128)(2,1)}, bf16[96,1024]{1,0:T(8,128)(2,1)S(1)}, u32[]{:S(2)}, u32[]{:S(2)}) collective-permute-start(bf16[96,1024]{1,0:T(8,128)(2,1)} %get-tuple-element.22.refs_3_), channel_id=1, source_target_pairs={{0,32},{1,33},{2,34},{3,35},{4,36},{5,37},{6,38},{7,39},{8,40},{9,... | collective-permute-start | bytes 589832 | tf_op jit(solution)/shard_map/ppermute | solution.py:42
  33.6 2.1 %collective-permute-start.2 = (bf16[96,1024]{1,0:T(8,128)(2,1)}, bf16[96,1024]{1,0:T(8,128)(2,1)S(1)}, u32[]{:S(2)}, u32[]{:S(2)}) collective-permute-start(bf16[96,1024]{1,0:T(8,128)(2,1)} %get-tuple-element.22.refs_3_), channel_id=1, source_target_pairs={{0,96},{1,97},{2,98},{3,99},{4,100},{5,101},{6,102},{7,103},{8,104... | collective-permute-start | bytes 589832 | tf_op jit(solution)/shard_map/ppermute | solution.py:42
  35.6 2.7 %collective-permute-start.3 = (bf16[96,1024]{1,0:T(8,128)(2,1)}, bf16[96,1024]{1,0:T(8,128)(2,1)S(1)}, u32[]{:S(2)}, u32[]{:S(2)}) collective-permute-start(bf16[96,1024]{1,0:T(8,128)(2,1)} %get-tuple-element.22.refs_3_), channel_id=1, source_target_pairs={{0,24},{1,25},{2,26},{3,27},{4,28},{5,29},{6,30},{7,31},{8,16},{9,... | collective-permute-start | bytes 589832 | tf_op jit(solution)/shard_map/ppermute | solution.py:42
  38.3 4.9 %collective-permute-done.1.refs_4_ = bf16[96,1024]{1,0:T(8,128)(2,1)S(1)} collective-permute-done((bf16[96,1024]{1,0:T(8,128)(2,1)}, bf16[96,1024]{1,0:T(8,128)(2,1)S(1)}, u32[]{:S(2)}, u32[]{:S(2)}) %collective-permute-start.1) | collective-permute-done | bytes 196640 | tf_op jit(solution)/shard_map/ppermute | solution.py:42
  43.2 2.4 %collective-permute-start.4 = (bf16[96,1024]{1,0:T(8,128)(2,1)S(1)}, bf16[96,1024]{1,0:T(8,128)(2,1)}, u32[]{:S(2)}, u32[]{:S(2)}) collective-permute-start(bf16[96,1024]{1,0:T(8,128)(2,1)S(1)} %collective-permute-done.1.refs_4_), channel_id=1, source_target_pairs={{0,96},{1,97},{2,98},{3,99},{4,100},{5,101},{6,102},{7,103},{8,104... | collective-permute-start | bytes 589832 | tf_op jit(solution)/shard_map/ppermute | solution.py:42
  45.6 1.4 %collective-permute-start = (bf16[8,16,1152]{2,1,0:T(8,128)(2,1)S(1)}, bf16[8,16,1152]{2,1,0:T(8,128)(2,1)S(1)}, u32[]{:S(2)}, u32[]{:S(2)}) collective-permute-start(bf16[8,16,1152]{2,1,0:T(8,128)(2,1)S(1)} %all-to-all-done.near.refs_0_), channel_id=1, source_target_pairs={{0,8},{1,9},{2,10},{3,11},{4,12},{5,13},{6,14},{7,15},{8,0},{9,1},... | collective-permute-start | bytes 884744 | tf_op jit(solution)/shard_map/ppermute | solution.py:42
  47.0 0.0 collective-permute-done.2.refs_5_
  47.0 1.9 %collective-permute-start.5 = (bf16[96,1024]{1,0:T(8,128)(2,1)S(1)}, bf16[96,1024]{1,0:T(8,128)(2,1)}, u32[]{:S(2)}, u32[]{:S(2)}) collective-permute-start(bf16[96,1024]{1,0:T(8,128)(2,1)S(1)} %collective-permute-done.2.refs_5_), channel_id=1, source_target_pairs={{0,24},{1,25},{2,26},{3,27},{4,28},{5,29},{6,30},{7,31},{8,16},{9,... | collective-permute-start | bytes 589832 | tf_op jit(solution)/shard_map/ppermute | solution.py:42
  48.8 0.0 collective-permute-done.3.refs_6_
  48.8 0.6 collective-permute-start.6
  49.4 0.8 collective-permute-done.4.refs_7_
  50.2 2.9 %collective-permute-start.7 = (bf16[96,1024]{1,0:T(8,128)(2,1)}, bf16[96,1024]{1,0:T(8,128)(2,1)}, u32[]{:S(2)}, u32[]{:S(2)}) collective-permute-start(bf16[96,1024]{1,0:T(8,128)(2,1)} %collective-permute-done.4.refs_7_), channel_id=1, source_target_pairs={{0,24},{1,25},{2,26},{3,27},{4,28},{5,29},{6,30},{7,31},{8,16},{9,... | collective-permute-start | bytes 589832 | tf_op jit(solution)/shard_map/ppermute | solution.py:42
  53.1 0.0 all-to-all-done.1.arrived
  53.1 0.0 copy-done
  53.1 0.0 copy-done.1
  53.1 0.0 copy-done.2
  53.1 1.5 %experts.1 = bf16[16,16,1024]{2,1,0:T(8,128)(2,1)} custom-call(bf16[16,16,1024]{2,1,0:T(8,128)(2,1)S(1)} %all-to-all-done.1.arrived, bf16[1,1024,256]{2,1,0:T(8,128)(2,1)S(1)} %copy-done, bf16[1,1024,256]{2,1,0:T(8,128)(2,1)S(1)} %copy-done.1, bf16[1,256,1024]{2,1,0:T(8,128)(2,1)S(1)} %copy-done.2), custom_call_target="tpu_custom_call" | custom-call | flops 500000000 | bytes 3000000 | tf_op jit(solution)/shard_map/experts/pallas_call | solution.py:358
  54.6 4.2 %all-to-all-start.2 = ((bf16[16,16,1024]{2,1,0:T(8,128)(2,1)}), bf16[16,16,1024]{2,1,0:T(8,128)(2,1)S(1)}, u32[]{:S(2)}, u32[]{:S(2)}) async-start(bf16[16,16,1024]{2,1,0:T(8,128)(2,1)} %experts.1), calls=%async_computation.2 | async-start | bytes 1048576 | tf_op jit(solution)/shard_map/all_to_all | solution.py:490
  58.8 0.0 copy-start.6
  58.8 0.0 copy-start.7
  58.8 0.0 collective-permute-done.5.refs_8_
  58.8 0.0 collective-permute-done.6.refs_9_
  58.9 0.0 collective-permute-done.refs_1_
  58.9 0.0 collective-permute-done.7.refs_10_
  58.9 0.0 copy-done.3
  58.9 0.0 copy-done.5
  58.9 2.0 %dense.1 = (bf16[8,16,1024]{2,1,0:T(8,128)(2,1)S(1)}, bf16[8,16,1024]{2,1,0:T(8,128)(2,1)S(1)}) custom-call(bf16[8,16,1152]{2,1,0:T(8,128)(2,1)S(1)} %all-to-all-done.near.refs_0_, bf16[8,16,1152]{2,1,0:T(8,128)(2,1)S(1)} %collective-permute-done.refs_1_, f32[1,1024]{1,0:T(1,128)S(1)} %bitcast.6, bf16[96,1024]{1,0:T(8,128)(2,1)S(1)} %copy-done.3, ...), custom_call_target="tpu_custom_call" | custom-call | flops 500000000 | bytes 4000000 | tf_op jit(solution)/shard_map/dense/pallas_call | solution.py:395
  60.9 2.0 %collective-permute-start.8 = (bf16[8,16,1024]{2,1,0:T(8,128)(2,1)S(1)}, bf16[8,16,1024]{2,1,0:T(8,128)(2,1)S(1)}, u32[]{:S(2)}, u32[]{:S(2)}) collective-permute-start(bf16[8,16,1024]{2,1,0:T(8,128)(2,1)S(1)} %get-tuple-element.24), channel_id=1, source_target_pairs={{0,8},{1,9},{2,10},{3,11},{4,12},{5,13},{6,14},{7,15},{8,0},{9,1},... | collective-permute-start | bytes 786440 | tf_op jit(solution)/shard_map/ppermute | solution.py:42
  62.9 8.0 %collective-permute-done.8.other = bf16[8,16,1024]{2,1,0:T(8,128)(2,1)S(1)} collective-permute-done((bf16[8,16,1024]{2,1,0:T(8,128)(2,1)S(1)}, bf16[8,16,1024]{2,1,0:T(8,128)(2,1)S(1)}, u32[]{:S(2)}, u32[]{:S(2)}) %collective-permute-start.8) | collective-permute-done | bytes 262176 | tf_op jit(solution)/shard_map/ppermute | solution.py:42
  70.9 0.8 all-to-all-done.2.back
  71.7 0.3 combine.1
  72.0 0.0 copy-start.4
  72.0 0.1 collective-permute-start.9
  72.1 1.3 %collective-permute-done.9.came = bf16[64,1024]{1,0:T(8,128)(2,1)S(1)} collective-permute-done((bf16[64,1024]{1,0:T(8,128)(2,1)S(1)}, bf16[64,1024]{1,0:T(8,128)(2,1)S(1)}, u32[]{:S(2)}, u32[]{:S(2)}) %collective-permute-start.9) | collective-permute-done | bytes 131104 | tf_op jit(solution)/shard_map/ppermute | solution.py:42
  73.4 0.6 collective-permute-start.10
  74.1 3.7 %collective-permute-done.10.came = bf16[32,1024]{1,0:T(8,128)(2,1)S(1)} collective-permute-done((bf16[32,1024]{1,0:T(8,128)(2,1)S(1)}, bf16[32,1024]{1,0:T(8,128)(2,1)S(1)}, u32[]{:S(2)}, u32[]{:S(2)}) %collective-permute-start.10) | collective-permute-done | bytes 65568 | tf_op jit(solution)/shard_map/ppermute | solution.py:42
  77.8 1.2 %collective-permute-start.11 = (bf16[16,1024]{1,0:T(8,128)(2,1)S(1)}, bf16[16,1024]{1,0:T(8,128)(2,1)S(1)}, u32[]{:S(2)}, u32[]{:S(2)}) collective-permute-start(bf16[16,1024]{1,0:T(8,128)(2,1)S(1)} %get-tuple-element.30), channel_id=1, source_target_pairs={{0,6},{1,7},{2,4},{3,5},{4,2},{5,3},{6,0},{7,1},{8,14},{9,15},{10,... | collective-permute-start | bytes 98312 | tf_op jit(solution)/shard_map/ppermute | solution.py:42
  79.0 0.0 copy-done.6
  79.0 0.0 copy-done.7
  79.0 0.0 copy-start.8
  79.0 1.0 %copy-done.8 = bf16[256,1024]{1,0:T(8,128)(2,1)S(1)} copy-done((bf16[256,1024]{1,0:T(8,128)(2,1)S(1)}, bf16[256,1024]{1,0:T(8,128)(2,1)}, u32[]{:S(2)}) %copy-start.8) | copy-done | bytes 524312
  80.1 0.0 copy-start.9
  80.1 0.8 copy-done.9
  80.8 0.4 shared.1.extra
  81.2 1.7 %collective-permute-done.11.came = bf16[16,1024]{1,0:T(8,128)(2,1)S(1)} collective-permute-done((bf16[16,1024]{1,0:T(8,128)(2,1)S(1)}, bf16[16,1024]{1,0:T(8,128)(2,1)S(1)}, u32[]{:S(2)}, u32[]{:S(2)}) %collective-permute-start.11) | collective-permute-done | bytes 32800 | tf_op jit(solution)/shard_map/ppermute | solution.py:42
  83.0 0.0 copy-done.4
  83.0 0.7 final.1
  (2 shorter events, 0.0 us)
Async XLA Ops:
  9.6 43.5 %copy-start = (bf16[1,1024,256]{2,1,0:T(8,128)(2,1)S(1)}, bf16[1,1024,256]{2,1,0:T(8,128)(2,1)}, u32[]{:S(2)}) copy-start(bf16[1,1024,256]{2,1,0:T(8,128)(2,1)} %gate.1) | copy-start | bytes 1572868
  9.6 43.5 %copy-start.1 = (bf16[1,1024,256]{2,1,0:T(8,128)(2,1)S(1)}, bf16[1,1024,256]{2,1,0:T(8,128)(2,1)}, u32[]{:S(2)}) copy-start(bf16[1,1024,256]{2,1,0:T(8,128)(2,1)} %up.1) | copy-start | bytes 1572868
  9.6 43.4 %copy-start.2 = (bf16[1,256,1024]{2,1,0:T(8,128)(2,1)S(1)}, bf16[1,256,1024]{2,1,0:T(8,128)(2,1)}, u32[]{:S(2)}) copy-start(bf16[1,256,1024]{2,1,0:T(8,128)(2,1)} %down.1) | copy-start | bytes 1572868
  9.7 12.4 %all-to-all-start = ((bf16[8,16,1152]{2,1,0:T(8,128)(2,1)}), bf16[8,16,1152]{2,1,0:T(8,128)(2,1)S(1)}, u32[]{:S(2)}, u32[]{:S(2)}) async-start(bf16[8,16,1152]{2,1,0:T(8,128)(2,1)} %get-tuple-element.19), calls=%async_computation | async-start | bytes 589824 | tf_op jit(solution)/shard_map/all_to_all | solution.py:490
  23.5 29.6 %all-to-all-start.1 = ((bf16[16,16,1024]{2,1,0:T(8,128)(2,1)}), bf16[16,16,1024]{2,1,0:T(8,128)(2,1)S(1)}, u32[]{:S(2)}, u32[]{:S(2)}) async-start(bf16[16,16,1024]{2,1,0:T(8,128)(2,1)} %get-tuple-element.20), calls=%async_computation.1 | async-start | bytes 1048576 | tf_op jit(solution)/shard_map/all_to_all | solution.py:490
  31.6 27.3 %copy-start.3 = (bf16[96,1024]{1,0:T(8,128)(2,1)S(1)}, bf16[96,1024]{1,0:T(8,128)(2,1)}, u32[]{:S(2)}) copy-start(bf16[96,1024]{1,0:T(8,128)(2,1)} %get-tuple-element.22.refs_3_) | copy-start | bytes 589828
  31.6 27.3 %copy-start.5 = (f32[1024]{0:T(1024)S(1)}, f32[1024]{0:T(1024)}, u32[]{:S(2)}) copy-start(f32[1024]{0:T(1024)} %param.45) | copy-start | bytes 12292
  31.6 11.7 %collective-permute-start.1 = (bf16[96,1024]{1,0:T(8,128)(2,1)}, bf16[96,1024]{1,0:T(8,128)(2,1)S(1)}, u32[]{:S(2)}, u32[]{:S(2)}) collective-permute-start(bf16[96,1024]{1,0:T(8,128)(2,1)} %get-tuple-element.22.refs_3_), channel_id=1, source_target_pairs={{0,32},{1,33},{2,34},{3,35},{4,36},{5,37},{6,38},{7,39},{8,40},{9,... | collective-permute-start | bytes 589832 | tf_op jit(solution)/shard_map/ppermute | solution.py:42
  33.6 13.4 %collective-permute-start.2 = (bf16[96,1024]{1,0:T(8,128)(2,1)}, bf16[96,1024]{1,0:T(8,128)(2,1)S(1)}, u32[]{:S(2)}, u32[]{:S(2)}) collective-permute-start(bf16[96,1024]{1,0:T(8,128)(2,1)} %get-tuple-element.22.refs_3_), channel_id=1, source_target_pairs={{0,96},{1,97},{2,98},{3,99},{4,100},{5,101},{6,102},{7,103},{8,104... | collective-permute-start | bytes 589832 | tf_op jit(solution)/shard_map/ppermute | solution.py:42
  35.6 13.2 %collective-permute-start.3 = (bf16[96,1024]{1,0:T(8,128)(2,1)}, bf16[96,1024]{1,0:T(8,128)(2,1)S(1)}, u32[]{:S(2)}, u32[]{:S(2)}) collective-permute-start(bf16[96,1024]{1,0:T(8,128)(2,1)} %get-tuple-element.22.refs_3_), channel_id=1, source_target_pairs={{0,24},{1,25},{2,26},{3,27},{4,28},{5,29},{6,30},{7,31},{8,16},{9,... | collective-permute-start | bytes 589832 | tf_op jit(solution)/shard_map/ppermute | solution.py:42
  43.2 7.0 %collective-permute-start.4 = (bf16[96,1024]{1,0:T(8,128)(2,1)S(1)}, bf16[96,1024]{1,0:T(8,128)(2,1)}, u32[]{:S(2)}, u32[]{:S(2)}) collective-permute-start(bf16[96,1024]{1,0:T(8,128)(2,1)S(1)} %collective-permute-done.1.refs_4_), channel_id=1, source_target_pairs={{0,96},{1,97},{2,98},{3,99},{4,100},{5,101},{6,102},{7,103},{8,104... | collective-permute-start | bytes 589832 | tf_op jit(solution)/shard_map/ppermute | solution.py:42
  45.6 13.3 %collective-permute-start = (bf16[8,16,1152]{2,1,0:T(8,128)(2,1)S(1)}, bf16[8,16,1152]{2,1,0:T(8,128)(2,1)S(1)}, u32[]{:S(2)}, u32[]{:S(2)}) collective-permute-start(bf16[8,16,1152]{2,1,0:T(8,128)(2,1)S(1)} %all-to-all-done.near.refs_0_), channel_id=1, source_target_pairs={{0,8},{1,9},{2,10},{3,11},{4,12},{5,13},{6,14},{7,15},{8,0},{9,1},... | collective-permute-start | bytes 884744 | tf_op jit(solution)/shard_map/ppermute | solution.py:42
  47.0 11.9 %collective-permute-start.5 = (bf16[96,1024]{1,0:T(8,128)(2,1)S(1)}, bf16[96,1024]{1,0:T(8,128)(2,1)}, u32[]{:S(2)}, u32[]{:S(2)}) collective-permute-start(bf16[96,1024]{1,0:T(8,128)(2,1)S(1)} %collective-permute-done.2.refs_5_), channel_id=1, source_target_pairs={{0,24},{1,25},{2,26},{3,27},{4,28},{5,29},{6,30},{7,31},{8,16},{9,... | collective-permute-start | bytes 589832 | tf_op jit(solution)/shard_map/ppermute | solution.py:42
  48.8 10.0 %collective-permute-start.6 = (bf16[96,1024]{1,0:T(8,128)(2,1)S(1)}, bf16[96,1024]{1,0:T(8,128)(2,1)}, u32[]{:S(2)}, u32[]{:S(2)}) collective-permute-start(bf16[96,1024]{1,0:T(8,128)(2,1)S(1)} %collective-permute-done.3.refs_6_), channel_id=1, source_target_pairs={{0,32},{1,33},{2,34},{3,35},{4,36},{5,37},{6,38},{7,39},{8,40},{9,... | collective-permute-start | bytes 589832 | tf_op jit(solution)/shard_map/ppermute | solution.py:42
  50.2 8.7 %collective-permute-start.7 = (bf16[96,1024]{1,0:T(8,128)(2,1)}, bf16[96,1024]{1,0:T(8,128)(2,1)}, u32[]{:S(2)}, u32[]{:S(2)}) collective-permute-start(bf16[96,1024]{1,0:T(8,128)(2,1)} %collective-permute-done.4.refs_7_), channel_id=1, source_target_pairs={{0,24},{1,25},{2,26},{3,27},{4,28},{5,29},{6,30},{7,31},{8,16},{9,... | collective-permute-start | bytes 589832 | tf_op jit(solution)/shard_map/ppermute | solution.py:42
  54.6 17.1 %all-to-all-start.2 = ((bf16[16,16,1024]{2,1,0:T(8,128)(2,1)}), bf16[16,16,1024]{2,1,0:T(8,128)(2,1)S(1)}, u32[]{:S(2)}, u32[]{:S(2)}) async-start(bf16[16,16,1024]{2,1,0:T(8,128)(2,1)} %experts.1), calls=%async_computation.2 | async-start | bytes 1048576 | tf_op jit(solution)/shard_map/all_to_all | solution.py:490
  58.8 20.2 %copy-start.6 = (bf16[1024,256]{1,0:T(8,128)(2,1)S(1)}, bf16[1024,256]{1,0:T(8,128)(2,1)}, u32[]{:S(2)}) copy-start(bf16[1024,256]{1,0:T(8,128)(2,1)} %s_gate.1) | copy-start | bytes 1572868
  58.8 20.2 %copy-start.7 = (bf16[1024,256]{1,0:T(8,128)(2,1)S(1)}, bf16[1024,256]{1,0:T(8,128)(2,1)}, u32[]{:S(2)}) copy-start(bf16[1024,256]{1,0:T(8,128)(2,1)} %s_up.1) | copy-start | bytes 1572868
  60.9 10.0 %collective-permute-start.8 = (bf16[8,16,1024]{2,1,0:T(8,128)(2,1)S(1)}, bf16[8,16,1024]{2,1,0:T(8,128)(2,1)S(1)}, u32[]{:S(2)}, u32[]{:S(2)}) collective-permute-start(bf16[8,16,1024]{2,1,0:T(8,128)(2,1)S(1)} %get-tuple-element.24), channel_id=1, source_target_pairs={{0,8},{1,9},{2,10},{3,11},{4,12},{5,13},{6,14},{7,15},{8,0},{9,1},... | collective-permute-start | bytes 786440 | tf_op jit(solution)/shard_map/ppermute | solution.py:42
  72.0 11.0 %copy-start.4 = (f32[16,1024]{1,0:T(8,128)S(1)}, f32[16,1024]{1,0:T(8,128)}, u32[]{:S(2)}) copy-start(f32[16,1024]{1,0:T(8,128)} %get-tuple-element.31.residual) | copy-start | bytes 196612
  72.0 1.4 %collective-permute-start.9 = (bf16[64,1024]{1,0:T(8,128)(2,1)S(1)}, bf16[64,1024]{1,0:T(8,128)(2,1)S(1)}, u32[]{:S(2)}, u32[]{:S(2)}) collective-permute-start(bf16[64,1024]{1,0:T(8,128)(2,1)S(1)} %get-tuple-element.26), channel_id=1, source_target_pairs={{0,1},{1,0},{2,3},{3,2},{4,5},{5,4},{6,7},{7,6},{8,9},{9,8},{10,11... | collective-permute-start | bytes 393224 | tf_op jit(solution)/shard_map/ppermute | solution.py:42
  73.4 4.3 %collective-permute-start.10 = (bf16[32,1024]{1,0:T(8,128)(2,1)S(1)}, bf16[32,1024]{1,0:T(8,128)(2,1)S(1)}, u32[]{:S(2)}, u32[]{:S(2)}) collective-permute-start(bf16[32,1024]{1,0:T(8,128)(2,1)S(1)} %get-tuple-element.28), channel_id=1, source_target_pairs={{0,2},{1,3},{2,0},{3,1},{4,6},{5,7},{6,4},{7,5},{8,10},{9,11},{10,... | collective-permute-start | bytes 196616 | tf_op jit(solution)/shard_map/ppermute | solution.py:42
  77.8 5.2 %collective-permute-start.11 = (bf16[16,1024]{1,0:T(8,128)(2,1)S(1)}, bf16[16,1024]{1,0:T(8,128)(2,1)S(1)}, u32[]{:S(2)}, u32[]{:S(2)}) collective-permute-start(bf16[16,1024]{1,0:T(8,128)(2,1)S(1)} %get-tuple-element.30), channel_id=1, source_target_pairs={{0,6},{1,7},{2,4},{3,5},{4,2},{5,3},{6,0},{7,1},{8,14},{9,15},{10,... | collective-permute-start | bytes 98312 | tf_op jit(solution)/shard_map/ppermute | solution.py:42
  79.0 1.0 %copy-start.8 = (bf16[256,1024]{1,0:T(8,128)(2,1)S(1)}, bf16[256,1024]{1,0:T(8,128)(2,1)}, u32[]{:S(2)}) copy-start(bf16[256,1024]{1,0:T(8,128)(2,1)} %s_down.1) | copy-start | bytes 1572868
  80.1 0.8 copy-start.9

commit v2 on v1

--- a/solution.py
+++ b/solution.py
@@ -224,9 +224,17 @@
             place < filled_of(s), found * jnp.exp(distance * rate_wide), 0.0
         ).astype(bf16)
 
+    def settle(found):
+        for s, inside, carried in found:
+            decay = jnp.exp((filled_of(s).astype(f32) + 1.0) * rate_tall)
+            both = jnp.where(value_block, inside + carried * decay, 0.0)
+            retained_s[s : s + 1, :] = jnp.sum(both, axis=0, keepdims=True)
+
+    pending = []
     for g in range(steps):
         for c in group_copies[g]:
             c.wait()
+        found = []
         for s in range(g * GROUP, (g + 1) * GROUP):
             inside = dot(weights_s[s], values[s])
             heads = blocked[s]
@@ -239,14 +247,16 @@
             carried = jnp.concatenate(
                 [dot(stacked, state[s, h].astype(bf16)) for h in range(HEADS)], axis=1
             )
-            decay = jnp.exp((filled_of(s).astype(f32) + 1.0) * rate_tall)
-            both = jnp.where(value_block, inside + carried * decay, 0.0)
-            retained_s[s : s + 1, :] = jnp.sum(both, axis=0, keepdims=True)
-
-    copies[8].wait()
+            found.append((s, inside, carried))
+        settle(pending)
+        pending = found
+        if g == 1:
+            copies[8].wait()
+            new_values = dot(normal_in, wv[...]).astype(bf16)
+            new_values_o[...] = new_values
+    settle(pending)
+
     copies[9].wait()
-    new_values = dot(normal_in, wv[...]).astype(bf16)
-    new_values_o[...] = new_values
     new_values32 = new_values.astype(f32)
     headed = []
     for h in range(HEADS):
@@ -373,13 +383,24 @@
     return found
 
 
+far_shards = (0, 4)
+
+
 def dense_kernel(*refs):
     near, other, mix = refs[0:3]
-    shards, own_o, other_o = refs[3:11], refs[11], refs[12]
+    shards, own_o, other_o = list(refs[3:11]), refs[11], refs[12]
+    held, sems = refs[13], refs[14]
+    copies = []
+    for i, k in enumerate(far_shards):
+        copies.append(pltpu.make_async_copy(shards[k], held.at[i], sems.at[i]))
+        copies[i].start()
+        shards[k] = held.at[i]
     count = NEAR * SEQ
     inputs = jnp.concatenate(
         [t[:, :, 0:WIDTH].reshape(count, WIDTH) for t in (near, other)], axis=0
     )
+    for c in copies:
+        c.wait()
     n = shards[0].shape[0] // 3
     gates, ups, downs = [
         jnp.concatenate([w[i * n : (i + 1) * n] for w in shards], axis=0) for i in range(3)
@@ -391,13 +412,21 @@
 
 
 def dense(near, other, weights, mix):
+    weights = [
+        pltpu.with_memory_space_constraint(w, pltpu.HBM) if k in far_shards else w
+        for k, w in enumerate(weights)
+    ]
     part = jax.ShapeDtypeStruct((NEAR, SEQ, WIDTH), bf16)
     return pl.pallas_call(
         dense_kernel,
         name="dense",
         out_shape=[part] * 2,
-        in_specs=[vmem] * 11,
+        in_specs=[vmem] * 3 + [hbm if k in far_shards else vmem for k in range(8)],
         out_specs=[vmem] * 2,
+        scratch_shapes=[
+            pltpu.VMEM((len(far_shards),) + weights[0].shape, bf16),
+            pltpu.SemaphoreType.DMA((len(far_shards),)),
+        ],
         cost_estimate=pl.CostEstimate(flops=500_000_000, bytes_accessed=4_000_000, transcendentals=0),
         compiler_params=pltpu.CompilerParams(vmem_limit_bytes=12 * MIB),
     )(near, other, mix[None], *weights)

time: 84.3 us -> 83.4 us (0.989)
  waiting for transfers between devices: 29.2 us -> 27.6 us
    pallas_call x1, Pallas kernels: 1.99 us -> 2.84 us  [dense(): pl.pallas_call(dense_kernel, name='dense', out_shape=[part] * 2, in_specs...]
    unnamed x20 -> x18, local copies, waits for them, and re-layouts: 1.85 us -> 1.84 us
  transfers between devices with their start and end apart: 15 -> 15, of which waited for: 8 -> 7; matrix products, arithmetic and copies ran while one was open for 0% -> 0% of each run, Pallas kernels for 5% -> 6%
where the time goes in v2:
time: 83.4 us; the launch traced here: 82.8 us
  starting transfers between devices  36.6 us (44%)
  waiting for transfers between devices  27.6 us (33%)
  Pallas kernels  16 us (19%)
  local copies, waits for them, and re-layouts  1.84 us (2%)
    ppermute x12, starting transfers between devices, flip(): lax.ppermute(values, 'ep', [(i, i ^ mask) for i in range(lax.axis_size('e...  19.8 us
    ppermute x12, waiting for transfers between devices, flip(): lax.ppermute(values, 'ep', [(i, i ^ mask) for i in range(lax.axis_size('e...  19.7 us
    all_to_all x3, starting transfers between devices, exchange(): lax.all_to_all(values, 'ep', split_axis=0, concat_axis=0, axis_index_grou...  16.8 us
    pallas_call x1, Pallas kernels, mixer(): pl.pallas_call(mixer_kernel, name='mixer', out_shape=shapes, in_specs=[hb...  8.81 us
    all_to_all x3, waiting for transfers between devices, exchange(): lax.all_to_all(values, 'ep', split_axis=0, concat_axis=0, axis_index_grou...  7.87 us
    pallas_call x1, Pallas kernels, dense(): pl.pallas_call(dense_kernel, name='dense', out_shape=[part] * 2, in_specs...  2.84 us
    unnamed x18, local copies, waits for them, and re-layouts  1.84 us
  transfers between devices with their start and end apart: 15, of which 7 were waited for; matrix products, arithmetic and copies ran while one was open for 0% of the time, Pallas kernels for 6%

profile of v2, /device:TPU:0, one launch (start us, length us, event | category | flops | bytes accessed | tf_op | source)
XLA Modules:
  0.0 82.8 jit_solution(11241092922797612881)
XLA Ops:
  0.6 8.8 %mixer.1 = (f32[16,1024]{1,0:T(8,128)}, bf16[16,1024]{1,0:T(8,128)(2,1)}, bf16[16,512]{1,0:T(8,128)(2,1)}, bf16[16,1024]{1,0:T(8,128)(2,1)}, bf16[8,16,1152]{2,1,0:T(8,128)(2,1)}, /*index=5*/bf16[96,1024]{1,0:T(8,128)(2,1)}) custom-call(s32[16]{0:T(128)} %lengths_h.1, s32[6,16]{1,0:T(8,128)} %bitcast.7, f32[6,16]{1,0:T(8,128)} %bitcast.8, ...), custom_call_target="tpu_custom_call" | custom-call | flops 2000000000 | bytes 22000000 | tf_op jit(solution)/shard_map/mixer/pallas_call | solution.py:293
  9.5 0.0 copy-start
  9.5 0.0 copy-start.1
  9.5 0.0 copy-start.2
  9.5 4.6 %all-to-all-start = ((bf16[8,16,1152]{2,1,0:T(8,128)(2,1)}), bf16[8,16,1152]{2,1,0:T(8,128)(2,1)S(1)}, u32[]{:S(2)}, u32[]{:S(2)}) async-start(bf16[8,16,1152]{2,1,0:T(8,128)(2,1)} %get-tuple-element.19), calls=%async_computation | async-start | bytes 589824 | tf_op jit(solution)/shard_map/all_to_all | solution.py:519
  14.0 7.9 %all-to-all-done.near.refs_0_ = bf16[8,16,1152]{2,1,0:T(8,128)(2,1)S(1)} async-done(((bf16[8,16,1152]{2,1,0:T(8,128)(2,1)}), bf16[8,16,1152]{2,1,0:T(8,128)(2,1)S(1)}, u32[]{:S(2)}, u32[]{:S(2)}) %all-to-all-start) | async-done | bytes 294944 | tf_op jit(solution)/shard_map/all_to_all | solution.py:519
  21.9 1.4 %select.1 = (bf16[16,16,1024]{2,1,0:T(8,128)(2,1)}, bf16[128,256]{1,0:T(8,128)(2,1)S(1)}) custom-call(s32[1]{0:T(128)} %bitcast.index.place, bf16[8,16,1152]{2,1,0:T(8,128)(2,1)S(1)} %all-to-all-done.near.refs_0_), custom_call_target="tpu_custom_call" | custom-call | tf_op jit(solution)/shard_map/select/pallas_call | solution.py:343
  23.3 8.0 %all-to-all-start.1 = ((bf16[16,16,1024]{2,1,0:T(8,128)(2,1)}), bf16[16,16,1024]{2,1,0:T(8,128)(2,1)S(1)}, u32[]{:S(2)}, u32[]{:S(2)}) async-start(bf16[16,16,1024]{2,1,0:T(8,128)(2,1)} %get-tuple-element.20), calls=%async_computation.1 | async-start | bytes 1048576 | tf_op jit(solution)/shard_map/all_to_all | solution.py:519
  31.4 0.0 copy-start.4
  31.4 2.0 %collective-permute-start.1 = (bf16[96,1024]{1,0:T(8,128)(2,1)}, bf16[96,1024]{1,0:T(8,128)(2,1)S(1)}, u32[]{:S(2)}, u32[]{:S(2)}) collective-permute-start(bf16[96,1024]{1,0:T(8,128)(2,1)} %get-tuple-element.22.refs_3_), channel_id=1, source_target_pairs={{0,32},{1,33},{2,34},{3,35},{4,36},{5,37},{6,38},{7,39},{8,40},{9,... | collective-permute-start | bytes 589832 | tf_op jit(solution)/shard_map/ppermute | solution.py:42
  33.4 2.1 %collective-permute-start.2 = (bf16[96,1024]{1,0:T(8,128)(2,1)}, bf16[96,1024]{1,0:T(8,128)(2,1)S(1)}, u32[]{:S(2)}, u32[]{:S(2)}) collective-permute-start(bf16[96,1024]{1,0:T(8,128)(2,1)} %get-tuple-element.22.refs_3_), channel_id=1, source_target_pairs={{0,96},{1,97},{2,98},{3,99},{4,100},{5,101},{6,102},{7,103},{8,104... | collective-permute-start | bytes 589832 | tf_op jit(solution)/shard_map/ppermute | solution.py:42
  35.5 2.7 %collective-permute-start.3 = (bf16[96,1024]{1,0:T(8,128)(2,1)}, bf16[96,1024]{1,0:T(8,128)(2,1)S(1)}, u32[]{:S(2)}, u32[]{:S(2)}) collective-permute-start(bf16[96,1024]{1,0:T(8,128)(2,1)} %get-tuple-element.22.refs_3_), channel_id=1, source_target_pairs={{0,24},{1,25},{2,26},{3,27},{4,28},{5,29},{6,30},{7,31},{8,16},{9,... | collective-permute-start | bytes 589832 | tf_op jit(solution)/shard_map/ppermute | solution.py:42
  38.2 4.9 %collective-permute-done.1.refs_4_ = bf16[96,1024]{1,0:T(8,128)(2,1)S(1)} collective-permute-done((bf16[96,1024]{1,0:T(8,128)(2,1)}, bf16[96,1024]{1,0:T(8,128)(2,1)S(1)}, u32[]{:S(2)}, u32[]{:S(2)}) %collective-permute-start.1) | collective-permute-done | bytes 196640 | tf_op jit(solution)/shard_map/ppermute | solution.py:42
  43.1 2.4 %collective-permute-start.4 = (bf16[96,1024]{1,0:T(8,128)(2,1)S(1)}, bf16[96,1024]{1,0:T(8,128)(2,1)}, u32[]{:S(2)}, u32[]{:S(2)}) collective-permute-start(bf16[96,1024]{1,0:T(8,128)(2,1)S(1)} %collective-permute-done.1.refs_4_), channel_id=1, source_target_pairs={{0,96},{1,97},{2,98},{3,99},{4,100},{5,101},{6,102},{7,103},{8,104... | collective-permute-start | bytes 589832 | tf_op jit(solution)/shard_map/ppermute | solution.py:42
  45.4 1.4 %collective-permute-start = (bf16[8,16,1152]{2,1,0:T(8,128)(2,1)S(1)}, bf16[8,16,1152]{2,1,0:T(8,128)(2,1)S(1)}, u32[]{:S(2)}, u32[]{:S(2)}) collective-permute-start(bf16[8,16,1152]{2,1,0:T(8,128)(2,1)S(1)} %all-to-all-done.near.refs_0_), channel_id=1, source_target_pairs={{0,8},{1,9},{2,10},{3,11},{4,12},{5,13},{6,14},{7,15},{8,0},{9,1},... | collective-permute-start | bytes 884744 | tf_op jit(solution)/shard_map/ppermute | solution.py:42
  46.8 0.0 collective-permute-done.2.refs_5_
  46.8 1.9 %collective-permute-start.5 = (bf16[96,1024]{1,0:T(8,128)(2,1)S(1)}, bf16[96,1024]{1,0:T(8,128)(2,1)S(1)}, u32[]{:S(2)}, u32[]{:S(2)}) collective-permute-start(bf16[96,1024]{1,0:T(8,128)(2,1)S(1)} %collective-permute-done.2.refs_5_), channel_id=1, source_target_pairs={{0,24},{1,25},{2,26},{3,27},{4,28},{5,29},{6,30},{7,31},{8,16},{9,... | collective-permute-start | bytes 589832 | tf_op jit(solution)/shard_map/ppermute | solution.py:42
  48.7 0.0 collective-permute-done.3.refs_6_
  48.7 0.6 collective-permute-start.6
  49.3 0.8 collective-permute-done.4.refs_7_
  50.1 2.9 %collective-permute-start.7 = (bf16[96,1024]{1,0:T(8,128)(2,1)}, bf16[96,1024]{1,0:T(8,128)(2,1)}, u32[]{:S(2)}, u32[]{:S(2)}) collective-permute-start(bf16[96,1024]{1,0:T(8,128)(2,1)} %collective-permute-done.4.refs_7_), channel_id=1, source_target_pairs={{0,24},{1,25},{2,26},{3,27},{4,28},{5,29},{6,30},{7,31},{8,16},{9,... | collective-permute-start | bytes 589832 | tf_op jit(solution)/shard_map/ppermute | solution.py:42
  52.9 0.0 all-to-all-done.1.arrived
  52.9 0.0 copy-done
  52.9 0.0 copy-done.1
  52.9 0.0 copy-done.2
  53.0 1.5 %experts.1 = bf16[16,16,1024]{2,1,0:T(8,128)(2,1)} custom-call(bf16[16,16,1024]{2,1,0:T(8,128)(2,1)S(1)} %all-to-all-done.1.arrived, bf16[1,1024,256]{2,1,0:T(8,128)(2,1)S(1)} %copy-done, bf16[1,1024,256]{2,1,0:T(8,128)(2,1)S(1)} %copy-done.1, bf16[1,256,1024]{2,1,0:T(8,128)(2,1)S(1)} %copy-done.2), custom_call_target="tpu_custom_call" | custom-call | flops 500000000 | bytes 3000000 | tf_op jit(solution)/shard_map/experts/pallas_call | solution.py:368
  54.5 4.2 %all-to-all-start.2 = ((bf16[16,16,1024]{2,1,0:T(8,128)(2,1)}), bf16[16,16,1024]{2,1,0:T(8,128)(2,1)S(1)}, u32[]{:S(2)}, u32[]{:S(2)}) async-start(bf16[16,16,1024]{2,1,0:T(8,128)(2,1)} %experts.1), calls=%async_computation.2 | async-start | bytes 1048576 | tf_op jit(solution)/shard_map/all_to_all | solution.py:519
  58.7 0.0 copy-start.5
  58.7 0.0 copy-start.6
  58.7 0.0 collective-permute-done.5.refs_8_
  58.7 0.0 collective-permute-done.6.refs_9_
  58.7 0.0 collective-permute-done.refs_1_
  58.7 0.0 collective-permute-done.7.refs_10_
  58.7 0.0 copy-done.4
  58.8 2.8 %dense.1 = (bf16[8,16,1024]{2,1,0:T(8,128)(2,1)S(1)}, bf16[8,16,1024]{2,1,0:T(8,128)(2,1)S(1)}) custom-call(bf16[8,16,1152]{2,1,0:T(8,128)(2,1)S(1)} %all-to-all-done.near.refs_0_, bf16[8,16,1152]{2,1,0:T(8,128)(2,1)S(1)} %collective-permute-done.refs_1_, f32[1,1024]{1,0:T(1,128)S(1)} %bitcast.6, bf16[96,1024]{1,0:T(8,128)(2,1)} %get-tuple-element.22.refs_3_, ...), custom_call_target="tpu_custom_call" | custom-call | flops 500000000 | bytes 4000000 | tf_op jit(solution)/shard_map/dense/pallas_call | solution.py:420
  61.6 2.0 %collective-permute-start.8 = (bf16[8,16,1024]{2,1,0:T(8,128)(2,1)S(1)}, bf16[8,16,1024]{2,1,0:T(8,128)(2,1)S(1)}, u32[]{:S(2)}, u32[]{:S(2)}) collective-permute-start(bf16[8,16,1024]{2,1,0:T(8,128)(2,1)S(1)} %get-tuple-element.24), channel_id=1, source_target_pairs={{0,8},{1,9},{2,10},{3,11},{4,12},{5,13},{6,14},{7,15},{8,0},{9,1},... | collective-permute-start | bytes 786440 | tf_op jit(solution)/shard_map/ppermute | solution.py:42
  63.6 7.2 %collective-permute-done.8.other = bf16[8,16,1024]{2,1,0:T(8,128)(2,1)S(1)} collective-permute-done((bf16[8,16,1024]{2,1,0:T(8,128)(2,1)S(1)}, bf16[8,16,1024]{2,1,0:T(8,128)(2,1)S(1)}, u32[]{:S(2)}, u32[]{:S(2)}) %collective-permute-start.8) | collective-permute-done | bytes 262176 | tf_op jit(solution)/shard_map/ppermute | solution.py:42
  70.8 0.0 all-to-all-done.2.back
  70.8 0.3 combine.1
  71.1 0.0 copy-start.3
  71.1 0.1 collective-permute-start.9
  71.2 1.3 %collective-permute-done.9.came = bf16[64,1024]{1,0:T(8,128)(2,1)S(1)} collective-permute-done((bf16[64,1024]{1,0:T(8,128)(2,1)S(1)}, bf16[64,1024]{1,0:T(8,128)(2,1)S(1)}, u32[]{:S(2)}, u32[]{:S(2)}) %collective-permute-start.9) | collective-permute-done | bytes 131104 | tf_op jit(solution)/shard_map/ppermute | solution.py:42
  72.5 0.6 collective-permute-start.10
  73.2 3.7 %collective-permute-done.10.came = bf16[32,1024]{1,0:T(8,128)(2,1)S(1)} collective-permute-done((bf16[32,1024]{1,0:T(8,128)(2,1)S(1)}, bf16[32,1024]{1,0:T(8,128)(2,1)S(1)}, u32[]{:S(2)}, u32[]{:S(2)}) %collective-permute-start.10) | collective-permute-done | bytes 65568 | tf_op jit(solution)/shard_map/ppermute | solution.py:42
  76.9 1.2 %collective-permute-start.11 = (bf16[16,1024]{1,0:T(8,128)(2,1)S(1)}, bf16[16,1024]{1,0:T(8,128)(2,1)S(1)}, u32[]{:S(2)}, u32[]{:S(2)}) collective-permute-start(bf16[16,1024]{1,0:T(8,128)(2,1)S(1)} %get-tuple-element.30), channel_id=1, source_target_pairs={{0,6},{1,7},{2,4},{3,5},{4,2},{5,3},{6,0},{7,1},{8,14},{9,15},{10,... | collective-permute-start | bytes 98312 | tf_op jit(solution)/shard_map/ppermute | solution.py:42
  78.1 0.0 copy-done.5
  78.1 0.0 copy-done.6
  78.1 0.0 copy-start.7
  78.1 1.0 %copy-done.7 = bf16[256,1024]{1,0:T(8,128)(2,1)S(1)} copy-done((bf16[256,1024]{1,0:T(8,128)(2,1)S(1)}, bf16[256,1024]{1,0:T(8,128)(2,1)}, u32[]{:S(2)}) %copy-start.7) | copy-done | bytes 524312
  79.2 0.0 copy-start.8
  79.2 0.8 copy-done.8
  79.9 0.4 shared.1.extra
  80.4 1.7 %collective-permute-done.11.came = bf16[16,1024]{1,0:T(8,128)(2,1)S(1)} collective-permute-done((bf16[16,1024]{1,0:T(8,128)(2,1)S(1)}, bf16[16,1024]{1,0:T(8,128)(2,1)S(1)}, u32[]{:S(2)}, u32[]{:S(2)}) %collective-permute-start.11) | collective-permute-done | bytes 32800 | tf_op jit(solution)/shard_map/ppermute | solution.py:42
  82.1 0.0 copy-done.3
  82.1 0.7 final.1
  (2 shorter events, 0.0 us)
Async XLA Ops:
  9.5 43.5 %copy-start = (bf16[1,1024,256]{2,1,0:T(8,128)(2,1)S(1)}, bf16[1,1024,256]{2,1,0:T(8,128)(2,1)}, u32[]{:S(2)}) copy-start(bf16[1,1024,256]{2,1,0:T(8,128)(2,1)} %gate.1) | copy-start | bytes 1572868
  9.5 43.5 %copy-start.1 = (bf16[1,1024,256]{2,1,0:T(8,128)(2,1)S(1)}, bf16[1,1024,256]{2,1,0:T(8,128)(2,1)}, u32[]{:S(2)}) copy-start(bf16[1,1024,256]{2,1,0:T(8,128)(2,1)} %up.1) | copy-start | bytes 1572868
  9.5 43.5 %copy-start.2 = (bf16[1,256,1024]{2,1,0:T(8,128)(2,1)S(1)}, bf16[1,256,1024]{2,1,0:T(8,128)(2,1)}, u32[]{:S(2)}) copy-start(bf16[1,256,1024]{2,1,0:T(8,128)(2,1)} %down.1) | copy-start | bytes 1572868
  9.5 12.4 %all-to-all-start = ((bf16[8,16,1152]{2,1,0:T(8,128)(2,1)}), bf16[8,16,1152]{2,1,0:T(8,128)(2,1)S(1)}, u32[]{:S(2)}, u32[]{:S(2)}) async-start(bf16[8,16,1152]{2,1,0:T(8,128)(2,1)} %get-tuple-element.19), calls=%async_computation | async-start | bytes 589824 | tf_op jit(solution)/shard_map/all_to_all | solution.py:519
  23.3 29.6 %all-to-all-start.1 = ((bf16[16,16,1024]{2,1,0:T(8,128)(2,1)}), bf16[16,16,1024]{2,1,0:T(8,128)(2,1)S(1)}, u32[]{:S(2)}, u32[]{:S(2)}) async-start(bf16[16,16,1024]{2,1,0:T(8,128)(2,1)} %get-tuple-element.20), calls=%async_computation.1 | async-start | bytes 1048576 | tf_op jit(solution)/shard_map/all_to_all | solution.py:519
  31.4 27.4 %copy-start.4 = (f32[1024]{0:T(1024)S(1)}, f32[1024]{0:T(1024)}, u32[]{:S(2)}) copy-start(f32[1024]{0:T(1024)} %param.45) | copy-start | bytes 12292
  31.4 11.7 %collective-permute-start.1 = (bf16[96,1024]{1,0:T(8,128)(2,1)}, bf16[96,1024]{1,0:T(8,128)(2,1)S(1)}, u32[]{:S(2)}, u32[]{:S(2)}) collective-permute-start(bf16[96,1024]{1,0:T(8,128)(2,1)} %get-tuple-element.22.refs_3_), channel_id=1, source_target_pairs={{0,32},{1,33},{2,34},{3,35},{4,36},{5,37},{6,38},{7,39},{8,40},{9,... | collective-permute-start | bytes 589832 | tf_op jit(solution)/shard_map/ppermute | solution.py:42
  33.4 13.4 %collective-permute-start.2 = (bf16[96,1024]{1,0:T(8,128)(2,1)}, bf16[96,1024]{1,0:T(8,128)(2,1)S(1)}, u32[]{:S(2)}, u32[]{:S(2)}) collective-permute-start(bf16[96,1024]{1,0:T(8,128)(2,1)} %get-tuple-element.22.refs_3_), channel_id=1, source_target_pairs={{0,96},{1,97},{2,98},{3,99},{4,100},{5,101},{6,102},{7,103},{8,104... | collective-permute-start | bytes 589832 | tf_op jit(solution)/shard_map/ppermute | solution.py:42
  35.5 13.2 %collective-permute-start.3 = (bf16[96,1024]{1,0:T(8,128)(2,1)}, bf16[96,1024]{1,0:T(8,128)(2,1)S(1)}, u32[]{:S(2)}, u32[]{:S(2)}) collective-permute-start(bf16[96,1024]{1,0:T(8,128)(2,1)} %get-tuple-element.22.refs_3_), channel_id=1, source_target_pairs={{0,24},{1,25},{2,26},{3,27},{4,28},{5,29},{6,30},{7,31},{8,16},{9,... | collective-permute-start | bytes 589832 | tf_op jit(solution)/shard_map/ppermute | solution.py:42
  43.1 7.0 %collective-permute-start.4 = (bf16[96,1024]{1,0:T(8,128)(2,1)S(1)}, bf16[96,1024]{1,0:T(8,128)(2,1)}, u32[]{:S(2)}, u32[]{:S(2)}) collective-permute-start(bf16[96,1024]{1,0:T(8,128)(2,1)S(1)} %collective-permute-done.1.refs_4_), channel_id=1, source_target_pairs={{0,96},{1,97},{2,98},{3,99},{4,100},{5,101},{6,102},{7,103},{8,104... | collective-permute-start | bytes 589832 | tf_op jit(solution)/shard_map/ppermute | solution.py:42
  45.4 13.3 %collective-permute-start = (bf16[8,16,1152]{2,1,0:T(8,128)(2,1)S(1)}, bf16[8,16,1152]{2,1,0:T(8,128)(2,1)S(1)}, u32[]{:S(2)}, u32[]{:S(2)}) collective-permute-start(bf16[8,16,1152]{2,1,0:T(8,128)(2,1)S(1)} %all-to-all-done.near.refs_0_), channel_id=1, source_target_pairs={{0,8},{1,9},{2,10},{3,11},{4,12},{5,13},{6,14},{7,15},{8,0},{9,1},... | collective-permute-start | bytes 884744 | tf_op jit(solution)/shard_map/ppermute | solution.py:42
  46.8 11.9 %collective-permute-start.5 = (bf16[96,1024]{1,0:T(8,128)(2,1)S(1)}, bf16[96,1024]{1,0:T(8,128)(2,1)S(1)}, u32[]{:S(2)}, u32[]{:S(2)}) collective-permute-start(bf16[96,1024]{1,0:T(8,128)(2,1)S(1)} %collective-permute-done.2.refs_5_), channel_id=1, source_target_pairs={{0,24},{1,25},{2,26},{3,27},{4,28},{5,29},{6,30},{7,31},{8,16},{9,... | collective-permute-start | bytes 589832 | tf_op jit(solution)/shard_map/ppermute | solution.py:42
  48.7 10.0 %collective-permute-start.6 = (bf16[96,1024]{1,0:T(8,128)(2,1)S(1)}, bf16[96,1024]{1,0:T(8,128)(2,1)}, u32[]{:S(2)}, u32[]{:S(2)}) collective-permute-start(bf16[96,1024]{1,0:T(8,128)(2,1)S(1)} %collective-permute-done.3.refs_6_), channel_id=1, source_target_pairs={{0,32},{1,33},{2,34},{3,35},{4,36},{5,37},{6,38},{7,39},{8,40},{9,... | collective-permute-start | bytes 589832 | tf_op jit(solution)/shard_map/ppermute | solution.py:42
  50.1 8.7 %collective-permute-start.7 = (bf16[96,1024]{1,0:T(8,128)(2,1)}, bf16[96,1024]{1,0:T(8,128)(2,1)}, u32[]{:S(2)}, u32[]{:S(2)}) collective-permute-start(bf16[96,1024]{1,0:T(8,128)(2,1)} %collective-permute-done.4.refs_7_), channel_id=1, source_target_pairs={{0,24},{1,25},{2,26},{3,27},{4,28},{5,29},{6,30},{7,31},{8,16},{9,... | collective-permute-start | bytes 589832 | tf_op jit(solution)/shard_map/ppermute | solution.py:42
  54.5 16.3 %all-to-all-start.2 = ((bf16[16,16,1024]{2,1,0:T(8,128)(2,1)}), bf16[16,16,1024]{2,1,0:T(8,128)(2,1)S(1)}, u32[]{:S(2)}, u32[]{:S(2)}) async-start(bf16[16,16,1024]{2,1,0:T(8,128)(2,1)} %experts.1), calls=%async_computation.2 | async-start | bytes 1048576 | tf_op jit(solution)/shard_map/all_to_all | solution.py:519
  58.7 19.5 %copy-start.5 = (bf16[1024,256]{1,0:T(8,128)(2,1)S(1)}, bf16[1024,256]{1,0:T(8,128)(2,1)}, u32[]{:S(2)}) copy-start(bf16[1024,256]{1,0:T(8,128)(2,1)} %s_gate.1) | copy-start | bytes 1572868
  58.7 19.4 %copy-start.6 = (bf16[1024,256]{1,0:T(8,128)(2,1)S(1)}, bf16[1024,256]{1,0:T(8,128)(2,1)}, u32[]{:S(2)}) copy-start(bf16[1024,256]{1,0:T(8,128)(2,1)} %s_up.1) | copy-start | bytes 1572868
  61.6 9.2 %collective-permute-start.8 = (bf16[8,16,1024]{2,1,0:T(8,128)(2,1)S(1)}, bf16[8,16,1024]{2,1,0:T(8,128)(2,1)S(1)}, u32[]{:S(2)}, u32[]{:S(2)}) collective-permute-start(bf16[8,16,1024]{2,1,0:T(8,128)(2,1)S(1)} %get-tuple-element.24), channel_id=1, source_target_pairs={{0,8},{1,9},{2,10},{3,11},{4,12},{5,13},{6,14},{7,15},{8,0},{9,1},... | collective-permute-start | bytes 786440 | tf_op jit(solution)/shard_map/ppermute | solution.py:42
  71.1 11.0 %copy-start.3 = (f32[16,1024]{1,0:T(8,128)S(1)}, f32[16,1024]{1,0:T(8,128)}, u32[]{:S(2)}) copy-start(f32[16,1024]{1,0:T(8,128)} %get-tuple-element.31.residual) | copy-start | bytes 196612
  71.1 1.4 %collective-permute-start.9 = (bf16[64,1024]{1,0:T(8,128)(2,1)S(1)}, bf16[64,1024]{1,0:T(8,128)(2,1)S(1)}, u32[]{:S(2)}, u32[]{:S(2)}) collective-permute-start(bf16[64,1024]{1,0:T(8,128)(2,1)S(1)} %get-tuple-element.26), channel_id=1, source_target_pairs={{0,1},{1,0},{2,3},{3,2},{4,5},{5,4},{6,7},{7,6},{8,9},{9,8},{10,11... | collective-permute-start | bytes 393224 | tf_op jit(solution)/shard_map/ppermute | solution.py:42
  72.5 4.3 %collective-permute-start.10 = (bf16[32,1024]{1,0:T(8,128)(2,1)S(1)}, bf16[32,1024]{1,0:T(8,128)(2,1)S(1)}, u32[]{:S(2)}, u32[]{:S(2)}) collective-permute-start(bf16[32,1024]{1,0:T(8,128)(2,1)S(1)} %get-tuple-element.28), channel_id=1, source_target_pairs={{0,2},{1,3},{2,0},{3,1},{4,6},{5,7},{6,4},{7,5},{8,10},{9,11},{10,... | collective-permute-start | bytes 196616 | tf_op jit(solution)/shard_map/ppermute | solution.py:42
  76.9 5.2 %collective-permute-start.11 = (bf16[16,1024]{1,0:T(8,128)(2,1)S(1)}, bf16[16,1024]{1,0:T(8,128)(2,1)S(1)}, u32[]{:S(2)}, u32[]{:S(2)}) collective-permute-start(bf16[16,1024]{1,0:T(8,128)(2,1)S(1)} %get-tuple-element.30), channel_id=1, source_target_pairs={{0,6},{1,7},{2,4},{3,5},{4,2},{5,3},{6,0},{7,1},{8,14},{9,15},{10,... | collective-permute-start | bytes 98312 | tf_op jit(solution)/shard_map/ppermute | solution.py:42
  78.1 1.0 %copy-start.7 = (bf16[256,1024]{1,0:T(8,128)(2,1)S(1)}, bf16[256,1024]{1,0:T(8,128)(2,1)}, u32[]{:S(2)}) copy-start(bf16[256,1024]{1,0:T(8,128)(2,1)} %s_down.1) | copy-start | bytes 1572868
  79.2 0.8 copy-start.8
